TPU v7x, 512 devices: a whole 4x8x8 slice. The times are simulated.
512 devices in a mesh: row: 32 (over z, x), col: 16 (over y, core).
Axes of the slice: x: 4, y: 8, z: 8, core: 2. Of those that a mesh axis runs over, the one named last changes fastest.
Arguments:
- tokens: bfloat16 [32768, 2048], P('row'), may hold values from -136 to 136
- norm_gain: float32 [2048], replicated, may hold values from 0.1 to 1.9
- w_in: bfloat16 [2048, 1024], P(None, 'col'), may hold values from -0.125 to 0.125
- w_out: bfloat16 [1024, 2048], P(None, 'col'), may hold values from -0.1875 to 0.1875
Outputs:
- mixed_tokens: bfloat16 [32768, 2048], P('row', 'col')
All inputs are finite; a program needn't handle non-finite values.
Results may differ from a plain program's by a relative error of at most 0.013.
Values may be sent and summed in bfloat16 or wider, within the bound.
No kernel may reach another device: no remote copies, remote signals or barrier semaphores. Data moves between devices by JAX's collectives and lax.ppermute only.
A program may use at most 64 MiB of HBM per device.

v0:
```python
import math

import jax
import jax.numpy as jnp
from jax import lax
from jax.sharding import PartitionSpec as P

GROUP = 256


NORM_EPS = 1e-06


def in_one_piece(arrays, axis, split_dim, concat_dim, along):
    ends, at = ([], 0)
    for a in arrays[:-1]:
        at += a.shape[along]
        ends.append(at)
    both = jnp.concatenate(arrays, axis=along)
    return tuple(
        jnp.split(
            lax.all_to_all(both, axis, split_axis=split_dim, concat_axis=concat_dim, tiled=True),
            ends,
            axis=along,
        )
    )


def as_sent(array):

    def short(part):
        return part.astype(jnp.bfloat16) if part.dtype == jnp.float32 else part

    return jax.tree.map(short, array)


def rotation_table(first_index, second_index, spectral_magnitude, factor):
    phase = (first_index * second_index % spectral_magnitude).astype(jnp.float32) * (
        2.0 * math.pi / spectral_magnitude
    )
    return (jnp.cos(phase) * factor, jnp.sin(phase) * factor)


def twiddle(real_input_values, imag_in, freq_index, pos_index, spectral_magnitude):
    cosine, sine = rotation_table(freq_index, pos_index, spectral_magnitude, 1.0)
    return (
        real_input_values * cosine + imag_in * sine,
        imag_in * cosine - real_input_values * sine,
    )


def second_section(stacked, half):
    length_dev = stacked.shape[1]
    stride = min(length_dev, 512)
    positions = lax.broadcasted_iota(jnp.int32, (length_dev, stride), 0)
    real_blocks = []
    imag_blocks = []
    for offset in range(0, length_dev, stride):
        freqs = lax.broadcasted_iota(jnp.int32, (length_dev, stride), 1) + offset
        cosine, sine = rotation_table(positions, freqs, length_dev, 1.0)
        with_cos = jnp.dot(stacked, cosine, precision=lax.Precision.HIGH)
        with_sin = jnp.dot(stacked, sine, precision=lax.Precision.HIGH)
        real_blocks.append(with_cos[:half] + with_sin[half:])
        imag_blocks.append(with_cos[half:] - with_sin[:half])
    return (jnp.concatenate(real_blocks, 1), jnp.concatenate(imag_blocks, 1))


def reorder_positions(arrived):
    channels, row_count, _, block_len = arrived.shape
    return jnp.swapaxes(arrived.reshape(channels, row_count, block_len), 1, 2).reshape(
        channels, row_count * block_len
    )


def local(tokens, norm_gain, w_in, w_out):
    length_dev = tokens.shape[0]
    row_count = lax.axis_size("row")
    col_count = lax.axis_size("col")
    total_len = length_dev * row_count
    widened = tokens.astype(jnp.float32)
    inverse = lax.rsqrt(jnp.mean(widened * widened, axis=1, keepdims=True) + NORM_EPS)
    normed = (widened * inverse * norm_gain[None, :]).astype(jnp.bfloat16)
    projected = lax.dot_general(
        w_in, normed, (((0,), (1,)), ((), ())), preferred_element_type=jnp.float32
    ).astype(jnp.bfloat16)
    channels = projected.shape[0]
    block_len = length_dev // row_count
    small_cos, small_sin = rotation_table(
        lax.broadcasted_iota(jnp.int32, (row_count, row_count), 0),
        lax.broadcasted_iota(jnp.int32, (row_count, row_count), 1),
        row_count,
        1.0 / math.sqrt(total_len),
    )
    per_row = channels // row_count
    arrived = lax.all_to_all(
        projected.reshape(channels, 1, length_dev), "row", split_axis=0, concat_axis=1, tiled=True
    )
    values = arrived.astype(jnp.float32)
    real_one = jnp.einsum("ka,cab->ckb", small_cos, values, precision=lax.Precision.HIGH)
    imag_one = -jnp.einsum("ka,cab->ckb", small_sin, values, precision=lax.Precision.HIGH)
    freq_index = lax.broadcasted_iota(jnp.int32, (row_count, length_dev), 0)
    pos_index = lax.broadcasted_iota(jnp.int32, (row_count, length_dev), 1)
    real_two, imag_two = twiddle(real_one, imag_one, freq_index, pos_index, total_len)
    stacked = jnp.concatenate(
        [
            real_two.reshape(per_row * row_count, length_dev),
            imag_two.reshape(per_row * row_count, length_dev),
        ],
        0,
    )
    real_three, imag_three = second_section(stacked, per_row * row_count)
    shaped = (per_row, row_count, row_count, block_len)
    back_real, back_imag = tuple(
        (
            part.astype(jnp.float32)
            for part in in_one_piece(
                (
                    real_three.reshape(shaped).astype(jnp.bfloat16),
                    imag_three.reshape(shaped).astype(jnp.bfloat16),
                ),
                "row",
                2,
                0,
                1,
            )
        )
    )
    spec_real = reorder_positions(back_real)
    spec_imag = reorder_positions(back_imag)
    quarter = length_dev // col_count
    group_cosine_table, group_sine_table = rotation_table(
        lax.broadcasted_iota(jnp.int32, (GROUP, GROUP), 0),
        lax.broadcasted_iota(jnp.int32, (GROUP, GROUP), 1),
        GROUP,
        1.0 / math.sqrt(GROUP),
    )
    real_input_values = lax.all_to_all(
        as_sent(spec_real.reshape(channels, col_count, quarter)),
        "col",
        split_axis=1,
        concat_axis=0,
        tiled=True,
    )
    imag_in = lax.all_to_all(
        as_sent(spec_imag.reshape(channels, col_count, quarter)),
        "col",
        split_axis=1,
        concat_axis=0,
        tiled=True,
    )
    width_all = real_input_values.shape[0]
    item_count = real_input_values.shape[2]
    groups = width_all // GROUP
    real_by_group = real_input_values.reshape(groups, GROUP, item_count)
    imaginary_by_group = imag_in.reshape(groups, GROUP, item_count)
    merged_spectrum = jnp.einsum(
        "hz,azo->aho", group_cosine_table, real_by_group, precision=lax.Precision.HIGH
    )
    merged_spectrum = merged_spectrum + jnp.einsum(
        "hz,azo->aho", group_sine_table, imaginary_by_group, precision=lax.Precision.HIGH
    )
    result = merged_spectrum.reshape(width_all, 1, item_count).astype(jnp.bfloat16)
    portion = lax.all_gather(result, "col", axis=2, tiled=True)
    flat = portion.reshape(portion.shape[0], portion.shape[2])
    output = lax.dot_general(
        flat, w_out, (((0,), (0,)), ((), ())), preferred_element_type=jnp.float32
    )
    return output.astype(jnp.bfloat16)


def solution(mesh):
    placed = (P("row", None), P(), P(None, "col"), P(None, "col"))
    return jax.shard_map(
        local, mesh=mesh, in_specs=placed, out_specs=P("row", "col"), check_vma=False
    )
```

profile of v0, /device:TPU:1, one launch (start us, length us, event | category | flops | bytes accessed | tf_op | source)
XLA Modules:
  0.0 170.5 jit_solution(13047247857492114618)
XLA Ops:
  6.5 3.2 %fusion = f32[1024]{0:T(1024)S(1)} fusion(bf16[1024,2048]{1,0:T(8,128)(2,1)} %param.4), kind=kLoop, calls=%fused_computation.2 | loop fusion | flops 6290432 | bytes 4198400 | tf_op jit(solution)/shard_map/reduce_sum | solution.py:81
  10.0 2.4 %fusion.38 = bf16[64,1,1024]{2,0,1:T(8,128)(2,1)S(1)} fusion(bf16[2048,64]{0,1:T(8,128)(2,1)} %param.6, bf16[1024,2048]{1,0:T(8,128)(2,1)S(1)} %copy-done.1, f32[2048]{0:T(1024)S(1)} %copy-done.2, f32[1024]{0:T(1024)S(1)} %add_rsqrt_fusion), kind=kOutput, calls=%fused_computation.44 | convolution fusion | flops 276889600 | bytes 4599808 | tf_op jit(solution)/shard_map/dot_general | solution.py:83
  12.4 0.5 broadcast.165
  13.0 0.7 reduce.1
  13.6 0.7 reshape.90
  14.3 13.9 %all-to-all-start = ((bf16[32,2,1024]{2,1,0:T(2,128)(2,1)}), bf16[32,2,1024]{2,1,0:T(2,128)(2,1)S(1)}, u32[]{:S(2)}, u32[]{:S(2)}) async-start(bf16[32,2,1024]{2,1,0:T(2,128)(2,1)} %reshape.90), calls=%async_computation | async-start | bytes 262144 | tf_op jit(solution)/shard_map/all_to_all | solution.py:95
  28.2 0.5 fusion.78
  28.8 8.6 %all-to-all-done = bf16[32,2,1024]{2,1,0:T(2,128)(2,1)S(1)} async-done(((bf16[32,2,1024]{2,1,0:T(2,128)(2,1)}), bf16[32,2,1024]{2,1,0:T(2,128)(2,1)S(1)}, u32[]{:S(2)}, u32[]{:S(2)}) %all-to-all-start) | async-done | bytes 131104 | tf_op jit(solution)/shard_map/all_to_all | solution.py:95
  37.5 0.7 reduce
  38.9 8.7 %fusion.21 = f32[128,512]{1,0:T(8,128)S(1)} fusion(f32[64,1024]{1,0:T(8,128)S(1)} %bitcast.98, f32[64,1024]{1,0:T(8,128)S(1)} %bitcast.94), kind=kOutput, calls=%fused_computation.28 | convolution fusion | flops 410124288 | bytes 786432 | tf_op jit(solution)/shard_map/dot_general | solution.py:62
  47.6 8.6 %fusion.17 = f32[128,512]{1,0:T(8,128)S(1)} fusion(s32[512]{0:T(512)S(1)} %iota_add_fusion, f32[64,1024]{1,0:T(8,128)S(1)} %bitcast.99, f32[64,1024]{1,0:T(8,128)S(1)} %bitcast.95), kind=kOutput, calls=%fused_computation.24 | convolution fusion | flops 410124288 | bytes 788480 | tf_op jit(solution)/shard_map/dot_general | solution.py:61
  56.2 8.9 %fusion.15 = f32[128,512]{1,0:T(8,128)S(1)} fusion(s32[512]{0:T(512)S(1)} %iota_add_fusion, f32[64,1024]{1,0:T(8,128)S(1)} %bitcast.100, f32[64,1024]{1,0:T(8,128)S(1)} %bitcast.96), kind=kOutput, calls=%fused_computation.22 | convolution fusion | flops 410124288 | bytes 788480 | tf_op jit(solution)/shard_map/dot_general | solution.py:62
  65.1 8.6 %fusion.23 = f32[128,512]{1,0:T(8,128)S(1)} fusion(f32[64,1024]{1,0:T(8,128)S(1)} %bitcast.101, f32[64,1024]{1,0:T(8,128)S(1)} %bitcast.97), kind=kOutput, calls=%fused_computation.30 | convolution fusion | flops 410124288 | bytes 786432 | tf_op jit(solution)/shard_map/dot_general | solution.py:61
  73.9 0.4 convert_element_type.108
  74.2 0.7 copy.35
  74.9 0.4 convert_element_type.107
  75.3 0.7 copy.34
  76.2 0.4 reshape.92
  76.6 13.7 %all_to_all.66 = bf16[32,2,2048]{2,1,0:T(2,128)(2,1)S(1)} all-to-all(bf16[32,2,2048]{2,1,0:T(2,128)(2,1)S(1)} %reshape.92), channel_id=1, replica_groups=mesh['row'=32,'col'=16] {'row'}, dimensions={0} | all-to-all | bytes 524288 | tf_op jit(solution)/shard_map/all_to_all | solution.py:22
  90.9 0.6 copy.41
  91.5 0.9 reshape.96
  92.4 10.9 %all-to-all-start.3 = ((bf16[16,2,2048]{2,1,0:T(2,128)(2,1)}), bf16[16,2,2048]{2,1,0:T(2,128)(2,1)S(1)}, u32[]{:S(2)}, u32[]{:S(2)}) async-start(bf16[16,2,2048]{2,1,0:T(2,128)(2,1)} %reshape.96), calls=%async_computation.3 | async-start | bytes 262144 | tf_op jit(solution)/shard_map/all_to_all | solution.py:144
  103.3 0.6 copy.37
  103.9 0.9 reshape.94
  104.8 7.4 %all-to-all-done.3 = bf16[16,2,2048]{2,1,0:T(2,128)(2,1)S(1)} async-done(((bf16[16,2,2048]{2,1,0:T(2,128)(2,1)}), bf16[16,2,2048]{2,1,0:T(2,128)(2,1)S(1)}, u32[]{:S(2)}, u32[]{:S(2)}) %all-to-all-start.3) | async-done | bytes 131104 | tf_op jit(solution)/shard_map/all_to_all | solution.py:144
  112.2 3.4 %all-to-all-start.2 = ((bf16[16,2,2048]{2,1,0:T(2,128)(2,1)}), bf16[16,2,2048]{2,1,0:T(2,128)(2,1)S(1)}, u32[]{:S(2)}, u32[]{:S(2)}) async-start(bf16[16,2,2048]{2,1,0:T(2,128)(2,1)} %reshape.94), calls=%async_computation.2 | async-start | bytes 262144 | tf_op jit(solution)/shard_map/all_to_all | solution.py:137
  116.3 8.2 %all-to-all-done.2 = bf16[16,2,2048]{2,1,0:T(2,128)(2,1)S(1)} async-done(((bf16[16,2,2048]{2,1,0:T(2,128)(2,1)}), bf16[16,2,2048]{2,1,0:T(2,128)(2,1)S(1)}, u32[]{:S(2)}, u32[]{:S(2)}) %all-to-all-start.2) | async-done | bytes 131104 | tf_op jit(solution)/shard_map/all_to_all | solution.py:137
  125.2 1.2 fusion.49
  126.4 1.2 fusion.37
  127.7 0.7 convert_element_type.118
  128.5 32.2 %all-gather.2.cloned.1.call-done = bf16[1024,1,1024]{0,2,1:T(8,128)(2,1)} async-done(((bf16[1024,1,64]{0,2,1:T(8,128)(2,1)}), bf16[1024,1,1024]{0,2,1:T(8,128)(2,1)}) %all-gather.2.cloned.1.call-update) | async-done | bytes 2097168 | tf_op jit(solution)/shard_map/all_gather | solution.py:163
  160.7 3.0 %fusion.29 = bf16[1024,128]{1,0:T(8,128)(2,1)} fusion(bf16[1024,128]{1,0:T(8,128)(2,1)S(1)} %copy-done, bf16[1024,1,1024]{0,2,1:T(8,128)(2,1)} %all-gather.2.cloned.1.call-done), kind=kOutput, calls=%fused_computation.36 | convolution fusion | flops 268566528 | bytes 2621440 | tf_op jit(solution)/shard_map/dot_general | solution.py:165
  (32 shorter events, 3.4 us)
Async XLA Ops:
  6.5 154.2 %copy-start = (bf16[1024,128]{1,0:T(8,128)(2,1)S(1)}, bf16[1024,128]{1,0:T(8,128)(2,1)}, u32[]{:S(2)}) copy-start(bf16[1024,128]{1,0:T(8,128)(2,1)} %param.7) | copy-start | bytes 786436
  6.5 3.5 %copy-start.1 = (bf16[1024,2048]{1,0:T(8,128)(2,1)S(1)}, bf16[1024,2048]{1,0:T(8,128)(2,1)}, u32[]{:S(2)}) copy-start(bf16[1024,2048]{1,0:T(8,128)(2,1)} %param.4) | copy-start | bytes 12582916
  6.5 3.5 %copy-start.2 = (f32[2048]{0:T(1024)S(1)}, f32[2048]{0:T(1024)}, u32[]{:S(2)}) copy-start(f32[2048]{0:T(1024)} %param.5) | copy-start | bytes 24580
  14.3 23.1 %all-to-all-start = ((bf16[32,2,1024]{2,1,0:T(2,128)(2,1)}), bf16[32,2,1024]{2,1,0:T(2,128)(2,1)S(1)}, u32[]{:S(2)}, u32[]{:S(2)}) async-start(bf16[32,2,1024]{2,1,0:T(2,128)(2,1)} %reshape.90), calls=%async_computation | async-start | bytes 262144 | tf_op jit(solution)/shard_map/all_to_all | solution.py:95
  92.4 19.8 %all-to-all-start.3 = ((bf16[16,2,2048]{2,1,0:T(2,128)(2,1)}), bf16[16,2,2048]{2,1,0:T(2,128)(2,1)S(1)}, u32[]{:S(2)}, u32[]{:S(2)}) async-start(bf16[16,2,2048]{2,1,0:T(2,128)(2,1)} %reshape.96), calls=%async_computation.3 | async-start | bytes 262144 | tf_op jit(solution)/shard_map/all_to_all | solution.py:144
  112.2 12.3 %all-to-all-start.2 = ((bf16[16,2,2048]{2,1,0:T(2,128)(2,1)}), bf16[16,2,2048]{2,1,0:T(2,128)(2,1)S(1)}, u32[]{:S(2)}, u32[]{:S(2)}) async-start(bf16[16,2,2048]{2,1,0:T(2,128)(2,1)} %reshape.94), calls=%async_computation.2 | async-start | bytes 262144 | tf_op jit(solution)/shard_map/all_to_all | solution.py:137
  115.6 45.1 %all-gather.2.cloned.1.call-start = ((), (), s32[]{:S(2)}) async-start(), calls=%async_computation.4 | async-start | bytes 2228224 | tf_op jit(solution)/shard_map/all_gather | solution.py:163
Sparse Core Ops, SparseCore 0:
  128.6 32.0 all-gather.1
where the time goes:
time: 171 us
  waiting for transfers between devices  56.5 us (33%)
  matrix products  43.2 us (25%)
  starting transfers between devices  28.2 us (16%)
  blocking collectives  13.7 us (8%)
  between operations  13.7 us (8%)
  local copies, waits for them, and re-layouts  9.71 us (6%)
  other arithmetic  5.56 us (3%)
    all_gather x1, waiting for transfers between devices, local(): portion = lax.all_gather(result, 'col', axis=2, tiled=True)  32.2 us
    dot_general x2, matrix products, second_section(): with_sin = jnp.dot(stacked, sine, precision=lax.Precision.HIGH)  17.6 us
    dot_general x2, matrix products, second_section(): with_cos = jnp.dot(stacked, cosine, precision=lax.Precision.HIGH)  17.2 us
    all_to_all x1, starting transfers between devices, local(): lax.all_to_all(projected.reshape(channels, 1, length_dev), 'row', split_a...  13.9 us
    all_to_all x1, blocking collectives, in_one_piece(): lax.all_to_all(both, axis, split_axis=split_dim, concat_axis=concat_dim,...  13.7 us
    all_to_all x1, starting transfers between devices, local(): lax.all_to_all(as_sent(spec_imag.reshape(channels, col_count, quarter)),...  10.9 us
    all_to_all x1, waiting for transfers between devices, local(): lax.all_to_all(projected.reshape(channels, 1, length_dev), 'row', split_a...  8.62 us
    all_to_all x1, waiting for transfers between devices, local(): lax.all_to_all(as_sent(spec_real.reshape(channels, col_count, quarter)),...  8.24 us
  transfers between devices with their start and end apart: 4, of which 4 were waited for; matrix products, arithmetic and copies ran while one was open for 2% of the time, Pallas kernels for 0%

commit v1 on v0

v1 whole, which is shorter than its diff:
```python
import math

import jax
import jax.numpy as jnp
import numpy as np
from jax import lax
from jax.experimental import pallas as pl
from jax.experimental.pallas import tpu as pltpu
from jax.sharding import Mesh
from jax.sharding import PartitionSpec as P

GROUP = 256
NORM_EPS = 1e-06
BLOCK = 128


def project_body(x_ref, w_ref, out_ref, scr):
    step = pl.program_id(0)
    x = x_ref[...]
    wide = x.astype(jnp.float32)
    inverse = lax.rsqrt(jnp.mean(wide * wide, axis=1, keepdims=True) + NORM_EPS)
    part = jnp.dot(x, w_ref[...], preferred_element_type=jnp.float32) * inverse
    turned = part.T
    half = turned.shape[0] // 2
    steps = pl.num_programs(0)
    scr[:, pl.ds(step, 1), :] = turned[:half].reshape(half, 1, BLOCK)
    scr[:, pl.ds(step + steps, 1), :] = turned[half:].reshape(half, 1, BLOCK)

    @pl.when(step == steps - 1)
    def _():
        out_ref[...] = scr[...].astype(jnp.bfloat16)


def project(tokens, weight):
    rows, width = tokens.shape
    channels = weight.shape[1]
    steps = rows // BLOCK
    shape = (channels // 2, 2 * steps, BLOCK)
    return pl.pallas_call(
        project_body,
        grid=(steps,),
        in_specs=[
            pl.BlockSpec((BLOCK, width), lambda s: (s, 0)),
            pl.BlockSpec((width, channels), lambda s: (0, 0)),
        ],
        out_specs=pl.BlockSpec(shape, lambda s: (0, 0, 0)),
        out_shape=jax.ShapeDtypeStruct(shape, jnp.bfloat16),
        scratch_shapes=[pltpu.VMEM(shape, jnp.float32)],
        compiler_params=pltpu.CompilerParams(dimension_semantics=("arbitrary",)),
    )(tokens, weight)


def fft_tables(total, n_first, n_second):
    scale = 1.0 / math.sqrt(total * GROUP)
    one = np.arange(n_first)
    two = np.arange(n_second)
    first = 2.0 * np.pi * (np.outer(one, one) % n_first) / n_first
    table_one = np.concatenate([np.cos(first), np.sin(first)], 0)
    turn = 2.0 * np.pi * np.outer(one, two) / total
    turns = np.stack([np.cos(turn), np.sin(turn)]) * scale
    second = 2.0 * np.pi * (np.outer(two, two) % n_second) / n_second
    cosine, sine = np.cos(second), np.sin(second)
    table_two = np.block([[cosine, sine], [-sine, cosine]])
    return (
        jnp.asarray(table_one, jnp.bfloat16),
        jnp.asarray(turns, jnp.float32),
        jnp.asarray(table_two, jnp.bfloat16),
    )


def positions_body(x_ref, one_ref, turn_ref, two_ref, out_ref, scr):
    wide = x_ref[...].astype(jnp.float32)
    n_first = wide.shape[0] * 8
    both = [
        wide[:, 8 * c : 8 * c + 8, :].reshape(n_first, BLOCK).astype(jnp.bfloat16)
        for c in range(2)
    ]
    cosine, sine = turn_ref[0], turn_ref[1]
    for c in range(2):
        y = jnp.dot(one_ref[...], both[c], preferred_element_type=jnp.float32)
        y_cos, y_sin = y[:n_first], y[n_first:]
        turned = jnp.concatenate(
            [y_cos * cosine - y_sin * sine, -(y_sin * cosine) - y_cos * sine], 1
        ).astype(jnp.bfloat16)
        z = lax.dot_general(
            two_ref[...], turned, (((1,), (1,)), ((), ())), preferred_element_type=jnp.float32
        )
        for part in range(2):
            for high in range(2):
                scr[:, 4 * c + 2 * part + high, :] = z[
                    BLOCK * part : BLOCK * part + BLOCK, BLOCK * high : BLOCK * high + BLOCK
                ]
    out_ref[...] = scr[...].astype(jnp.bfloat16)


def positions(arrived, total):
    rows = arrived.shape[0]
    tables = fft_tables(total, rows * 8, BLOCK)
    shape = (BLOCK, 8, BLOCK)
    return pl.pallas_call(
        positions_body,
        out_shape=jax.ShapeDtypeStruct(shape, jnp.bfloat16),
        scratch_shapes=[pltpu.VMEM(shape, jnp.float32)],
    )(arrived, *tables)


def channel_table(rows, near):
    source = np.arange(rows * near)
    channel = np.stack(
        [(GROUP // near) * (source % near) + source // near + rows * c for c in range(2)]
    )
    freq = np.arange(GROUP)
    phase = 2.0 * np.pi * (freq[:, None, None] * channel[None] % GROUP) / GROUP
    both = np.stack([np.cos(phase), np.sin(phase)], 2)
    return jnp.asarray(both.reshape(GROUP, -1), jnp.bfloat16)


def channels_body(x_ref, table_ref, out_ref, scr):
    scr[...] = x_ref[...].astype(jnp.float32)
    rows = [
        jnp.concatenate([scr[:, 2 * j, :], scr[:, 2 * j + 1, :]], 1).astype(jnp.bfloat16)
        for j in range(4)
    ]
    data = jnp.concatenate(rows, 0)
    spectrum = jnp.dot(table_ref[...], data, preferred_element_type=jnp.float32)
    out_ref[...] = spectrum.T.astype(jnp.bfloat16)


def channel_mix(arrived, table):
    count = arrived.shape[1] * arrived.shape[2] // 4
    return pl.pallas_call(
        channels_body,
        out_shape=jax.ShapeDtypeStruct((count, GROUP), jnp.bfloat16),
        scratch_shapes=[pltpu.VMEM(arrived.shape, jnp.float32)],
    )(arrived, table)


def output_body(half_ref, spec_ref, own_ref, other_ref, out_ref):
    half = half_ref[0]
    groups = spec_ref.shape[0]
    for k in range(2):
        for ref, place in ((own_ref, 2 * half + k), (other_ref, 2 * (1 - half) + k)):
            total = None
            for g in range(groups):
                part = jnp.dot(
                    spec_ref[g],
                    ref[k, GROUP * g : GROUP * g + GROUP, :],
                    preferred_element_type=jnp.float32,
                )
                total = part if total is None else total + part
            out_ref[pl.ds(place, 1)] = total.astype(jnp.bfloat16)[None]


def output_map(half, gathered, own, other):
    count = gathered.shape[1]
    return pl.pallas_call(
        output_body,
        in_specs=[
            pl.BlockSpec(memory_space=pltpu.SMEM),
            pl.BlockSpec(memory_space=pltpu.VMEM),
            pl.BlockSpec(memory_space=pltpu.VMEM),
            pl.BlockSpec(memory_space=pltpu.VMEM),
        ],
        out_shape=jax.ShapeDtypeStruct((4, count, own.shape[2]), jnp.bfloat16),
    )(half, gathered, own, other)


def local(tokens, norm_gain, w_in, w_out):
    rows = lax.axis_size("row")
    total = tokens.shape[0] * rows
    own = lax.all_gather(w_out, "k", axis=0)
    other = lax.ppermute(own, "h", [(0, 1), (1, 0)])
    weight = (w_in.astype(jnp.float32) * norm_gain[:, None]).astype(jnp.bfloat16)
    projected = project(tokens, weight)
    arrived = lax.all_to_all(projected, "row", 0, 0, tiled=True)
    spectra = positions(arrived, total)
    arrived = lax.all_to_all(spectra, ("row", "h", "k"), 0, 0, tiled=True)
    mixed = channel_mix(arrived, channel_table(rows, 4))
    gathered = lax.all_gather(mixed, "g", axis=0)
    half = lax.axis_index("h").astype(jnp.int32).reshape(1)
    output = output_map(half, gathered, own, other)
    output = lax.all_to_all(output, ("h", "k"), 0, 0, tiled=True)
    return output.reshape(tokens.shape[0], w_out.shape[1])


def solution(mesh):
    mesh = Mesh(mesh.devices.reshape(32, 4, 2, 2), ("row", "g", "h", "k"))
    columns = ("g", "h", "k")
    placed = (P("row", None), P(), P(None, columns), P(None, columns))
    return jax.shard_map(
        local, mesh=mesh, in_specs=placed, out_specs=P("row", columns), check_vma=False
    )
```

time: 171 us -> 93 us (0.54)
  waiting for transfers between devices: 56.5 us -> 8.18 us
  matrix products: 43.2 us -> 0 us
  blocking collectives: 13.7 us -> 53.9 us
  starting transfers between devices: 28.2 us -> 10.3 us
  Pallas kernels: 0 us -> 14.7 us
  between operations: 13.7 us -> 0.05 us
  local copies, waits for them, and re-layouts: 9.71 us -> 3.36 us
  other arithmetic: 5.56 us -> 1.87 us
    dot_general x10 -> x0, matrix products: 43.2 us -> none  [the longest x2 17.6 us: second_section(): with_sin = jnp.dot(stacked, sine, precision=lax.Precision.HIGH)]
    all_gather x1 -> x0, waiting for transfers between devices: 32.2 us -> none  [local(): portion = lax.all_gather(result, 'col', axis=2, tiled=True)]
    all_to_all x1 -> x2, blocking collectives: 13.7 us -> 34.6 us  [the longest x1 23.2 us: local(): arrived = lax.all_to_all(projected, 'row', 0, 0, tiled=True)]
    all_to_all x3 -> x1, starting transfers between devices: 28.2 us -> 7.55 us  [local(): arrived = lax.all_to_all(spectra, ('row', 'h', 'k'), 0, 0, tiled=True)]
    all_gather x0 -> x2, blocking collectives: none -> 19.3 us  [the longest x1 16.6 us: local(): gathered = lax.all_gather(mixed, 'g', axis=0)]
    all_to_all x3 -> x1, waiting for transfers between devices: 24.2 us -> 8.18 us  [local(): arrived = lax.all_to_all(spectra, ('row', 'h', 'k'), 0, 0, tiled=True)]
    pallas_call x0 -> x4, Pallas kernels: none -> 14.7 us  [the longest x1 6.95 us: project(): pl.pallas_call(project_body, grid=(steps,), in_specs=[pl.BlockSpec((BLOCK...]
    reduce_sum x1 -> x0, other arithmetic: 3.22 us -> none  [local(): jnp.mean(widened * widened, axis=1, keepdims=True) + NORM_EPS]
  transfers between devices with their start and end apart: 4 -> 2, of which waited for: 4 -> 1; matrix products, arithmetic and copies ran while one was open for 2% -> 0% of each run, Pallas kernels for 0% -> 2%
where the time goes in v1:
time: 93 us; the launch traced here: 92.4 us
  blocking collectives  53.9 us (58%)
  Pallas kernels  14.7 us (16%)
  starting transfers between devices  10.3 us (11%)
  waiting for transfers between devices  8.18 us (9%)
  local copies, waits for them, and re-layouts  3.36 us (4%)
  other arithmetic  1.87 us (2%)
    all_to_all x1, blocking collectives, local(): arrived = lax.all_to_all(projected, 'row', 0, 0, tiled=True)  23.2 us
    all_gather x1, blocking collectives, local(): gathered = lax.all_gather(mixed, 'g', axis=0)  16.6 us
    all_to_all x1, blocking collectives, local(): output = lax.all_to_all(output, ('h', 'k'), 0, 0, tiled=True)  11.4 us
    all_to_all x1, waiting for transfers between devices, local(): arrived = lax.all_to_all(spectra, ('row', 'h', 'k'), 0, 0, tiled=True)  8.18 us
    all_to_all x1, starting transfers between devices, local(): arrived = lax.all_to_all(spectra, ('row', 'h', 'k'), 0, 0, tiled=True)  7.55 us
    pallas_call x1, Pallas kernels, project(): pl.pallas_call(project_body, grid=(steps,), in_specs=[pl.BlockSpec((BLOCK...  6.95 us
    pallas_call x1, Pallas kernels, positions(): pl.pallas_call(positions_body, out_shape=jax.ShapeDtypeStruct(shape, jnp....  2.79 us
    pallas_call x1, Pallas kernels, output_map(): pl.pallas_call(output_body, in_specs=[pl.BlockSpec(memory_space=pltpu.SME...  2.76 us
  transfers between devices with their start and end apart: 2, of which 1 were waited for; matrix products, arithmetic and copies ran while one was open for 0% of the time, Pallas kernels for 2%

profile of v1, /device:TPU:1, one launch (start us, length us, event | category | flops | bytes accessed | tf_op | source)
XLA Modules:
  0.0 92.4 jit_solution(10344827322712380164)
XLA Ops:
  0.0 1.2 %copy.10 = f32[2048,64]{1,0:T(8,128)S(1)} copy(bf16[2048,64]{0,1:T(8,128)(2,1)} %param.10) | data formatting | bytes 786432 | tf_op jit(solution)/shard_map/convert_element_type | solution.py:173
  1.2 0.0 copy-start.3
  1.2 1.9 %multiply_convert_fusion.w_ref = bf16[2048,64]{1,0:T(8,128)(2,1)} fusion(f32[2048,64]{1,0:T(8,128)S(1)} %copy.10, f32[2048]{0:T(1024)} %param.9), kind=kLoop, calls=%fused_computation | loop fusion | flops 262144 | bytes 794624 | tf_op jit(solution)/shard_map/convert_element_type | solution.py:173
  3.0 7.0 %shard_map.82 = bf16[32,16,128]{2,1,0:T(8,128)(2,1)} custom-call(bf16[1024,2048]{1,0:T(8,128)(2,1)} %x_ref.1, bf16[2048,64]{1,0:T(8,128)(2,1)} %multiply_convert_fusion.w_ref), custom_call_target="tpu_custom_call" | custom-call | tf_op jit(solution)/shard_map/pallas_call | solution.py:39
  10.0 23.2 %all_to_all.15.x_ref = bf16[32,16,128]{2,1,0:T(8,128)(2,1)} all-to-all(bf16[32,16,128]{2,1,0:T(8,128)(2,1)} %shard_map.82), channel_id=1, replica_groups=mesh['row'=32,'g'=4,'h'=2,'k'=2] {'row'}, dimensions={0} | all-to-all | bytes 262144 | tf_op jit(solution)/shard_map/all_to_all | solution.py:175
  33.1 2.8 %shard_map.83 = bf16[128,8,128]{2,1,0:T(8,128)(2,1)} custom-call(bf16[32,16,128]{2,1,0:T(8,128)(2,1)} %all_to_all.15.x_ref, bf16[512,256]{1,0:T(8,128)(2,1)} %constant.12.clone.one_ref, f32[2,256,128]{2,1,0:T(8,128)} %constant.13.clone.turn_ref, bf16[256,256]{1,0:T(8,128)(2,1)} %constant.14.clone.two_ref), custom_call_target="tpu_custom_call" | custom-call | tf_op jit(solution)/shard_map/pallas_call | solution.py:100
  35.9 7.5 %all-to-all-start.1 = ((bf16[128,8,128]{2,1,0:T(8,128)(2,1)}), bf16[128,8,128]{2,1,0:T(8,128)(2,1)S(1)}, u32[]{:S(2)}, u32[]{:S(2)}) async-start(bf16[128,8,128]{2,1,0:T(8,128)(2,1)} %shard_map.83), calls=%async_computation.1 | async-start | bytes 524288 | tf_op jit(solution)/shard_map/all_to_all | solution.py:177
  43.5 0.0 copy-done.3
  43.5 2.7 %all-gather.1 = bf16[2048,128]{1,0:T(8,128)(2,1)S(1)} all-gather(bf16[1024,128]{1,0:T(8,128)(2,1)S(1)} %copy-done.3), channel_id=3, replica_groups=mesh['row'=32,'g'=4,'h'=2,'k'=2] {'k'}, dimensions={0}, use_global_device_ids=true | all-gather | bytes 786432 | tf_op jit(solution)/shard_map/all_gather | solution.py:171
  46.2 0.0 copy-start
  46.2 2.7 %collective-permute-start = (bf16[2,1024,128]{2,1,0:T(8,128)(2,1)S(1)}, bf16[2,1024,128]{2,1,0:T(8,128)(2,1)S(1)}, u32[]{:S(2)}, u32[]{:S(2)}) collective-permute-start(bf16[2,1024,128]{2,1,0:T(8,128)(2,1)S(1)} %bitcast.5), channel_id=1, source_target_pairs={{0,2},{2,0},{1,3},{3,1},{4,6},{6,4},{5,7},{7,5},{8,10},{10,8},{9,1... | collective-permute-start | bytes 1572872 | tf_op jit(solution)/shard_map/ppermute | solution.py:172
  49.0 8.2 %all-to-all-done.1.x_ref = bf16[128,8,128]{2,1,0:T(8,128)(2,1)S(1)} async-done(((bf16[128,8,128]{2,1,0:T(8,128)(2,1)}), bf16[128,8,128]{2,1,0:T(8,128)(2,1)S(1)}, u32[]{:S(2)}, u32[]{:S(2)}) %all-to-all-start.1) | async-done | bytes 262176 | tf_op jit(solution)/shard_map/all_to_all | solution.py:177
  57.2 0.0 copy-start.1
  57.2 0.7 copy-done.1
  57.9 2.2 %shard_map.84 = bf16[256,256]{1,0:T(8,128)(2,1)} custom-call(bf16[128,8,128]{2,1,0:T(8,128)(2,1)} %copy-done.1, bf16[256,512]{1,0:T(8,128)(2,1)} %constant.15.clone.table_ref), custom_call_target="tpu_custom_call" | custom-call | tf_op jit(solution)/shard_map/pallas_call | solution.py:131
  60.1 16.6 %all-gather = bf16[1024,256]{1,0:T(8,128)(2,1)} all-gather(bf16[256,256]{1,0:T(8,128)(2,1)} %shard_map.84), channel_id=2, replica_groups=mesh['row'=32,'g'=4,'h'=2,'k'=2] {'g'}, dimensions={0}, use_global_device_ids=true | all-gather | bytes 655360 | tf_op jit(solution)/shard_map/all_gather | solution.py:179
  76.7 0.0 collective-permute-done.other_ref
  76.7 0.0 copy-start.2
  76.7 0.0 copy-done
  76.7 0.8 copy-done.2
  77.5 2.8 %shard_map.85 = bf16[4,256,128]{2,1,0:T(8,128)(2,1)} custom-call(s32[1]{0:T(128)} %bitcast.half_ref, bf16[4,256,256]{2,1,0:T(8,128)(2,1)} %bitcast.4, bf16[2,1024,128]{2,1,0:T(8,128)(2,1)} %bitcast.6, bf16[2,1024,128]{2,1,0:T(8,128)(2,1)} %copy-done.2), custom_call_target="tpu_custom_call" | custom-call | tf_op jit(solution)/shard_map/pallas_call | solution.py:156
  80.2 11.4 %all_to_all.16 = bf16[4,256,128]{2,1,0:T(8,128)(2,1)S(1)} all-to-all(bf16[4,256,128]{2,1,0:T(8,128)(2,1)} %shard_map.85), channel_id=1, replica_groups=mesh['row'=32,'g'=4,'h'=2,'k'=2] {'h','k'}, dimensions={0} | all-to-all | bytes 524288 | tf_op jit(solution)/shard_map/all_to_all | solution.py:182
  91.7 0.7 copy.12
Async XLA Ops:
  1.2 42.3 %copy-start.3 = (bf16[1024,128]{1,0:T(8,128)(2,1)S(1)}, bf16[1024,128]{1,0:T(8,128)(2,1)}, u32[]{:S(2)}) copy-start(bf16[1024,128]{1,0:T(8,128)(2,1)} %param.11) | copy-start | bytes 786436
  35.9 21.2 %all-to-all-start.1 = ((bf16[128,8,128]{2,1,0:T(8,128)(2,1)}), bf16[128,8,128]{2,1,0:T(8,128)(2,1)S(1)}, u32[]{:S(2)}, u32[]{:S(2)}) async-start(bf16[128,8,128]{2,1,0:T(8,128)(2,1)} %shard_map.83), calls=%async_computation.1 | async-start | bytes 524288 | tf_op jit(solution)/shard_map/all_to_all | solution.py:177
  46.2 30.5 %copy-start = (bf16[2048,128]{1,0:T(8,128)(2,1)}, bf16[2048,128]{1,0:T(8,128)(2,1)S(1)}, u32[]{:S(2)}) copy-start(bf16[2048,128]{1,0:T(8,128)(2,1)S(1)} %all-gather.1) | copy-start | bytes 1572868
  46.2 30.5 %collective-permute-start = (bf16[2,1024,128]{2,1,0:T(8,128)(2,1)S(1)}, bf16[2,1024,128]{2,1,0:T(8,128)(2,1)S(1)}, u32[]{:S(2)}, u32[]{:S(2)}) collective-permute-start(bf16[2,1024,128]{2,1,0:T(8,128)(2,1)S(1)} %bitcast.5), channel_id=1, source_target_pairs={{0,2},{2,0},{1,3},{3,1},{4,6},{6,4},{5,7},{7,5},{8,10},{10,8},{9,1... | collective-permute-start | bytes 1572872 | tf_op jit(solution)/shard_map/ppermute | solution.py:172
  57.2 0.7 copy-start.1
  76.7 0.8 copy-start.2

commit v2 on v1

--- a/solution.py
+++ b/solution.py
@@ -12,42 +12,61 @@
 GROUP = 256
 NORM_EPS = 1e-06
 BLOCK = 128
-
-
-def project_body(x_ref, w_ref, out_ref, scr):
-    step = pl.program_id(0)
-    x = x_ref[...]
-    wide = x.astype(jnp.float32)
-    inverse = lax.rsqrt(jnp.mean(wide * wide, axis=1, keepdims=True) + NORM_EPS)
-    part = jnp.dot(x, w_ref[...], preferred_element_type=jnp.float32) * inverse
-    turned = part.T
-    half = turned.shape[0] // 2
-    steps = pl.num_programs(0)
-    scr[:, pl.ds(step, 1), :] = turned[:half].reshape(half, 1, BLOCK)
-    scr[:, pl.ds(step + steps, 1), :] = turned[half:].reshape(half, 1, BLOCK)
-
-    @pl.when(step == steps - 1)
-    def _():
-        out_ref[...] = scr[...].astype(jnp.bfloat16)
-
-
-def project(tokens, weight):
+SMALL = pltpu.CompilerParams(vmem_limit_bytes=16 << 20)
+
+
+def project_body(x_hbm, w_hbm, gain_hbm, out_ref, x_buf, w_buf, gain_buf, scr, sems):
+    pieces = sems.shape[0] - 2
+    rows = x_buf.shape[0] // pieces
+    weights = pltpu.make_async_copy(w_hbm, w_buf, sems.at[pieces])
+    gains = pltpu.make_async_copy(gain_hbm, gain_buf, sems.at[pieces + 1])
+    weights.start()
+    gains.start()
+    copies = []
+    for j in range(pieces):
+        span = pl.ds(rows * j, rows)
+        copies.append(pltpu.make_async_copy(x_hbm.at[span], x_buf.at[span], sems.at[j]))
+        copies[j].start()
+    weights.wait()
+    gains.wait()
+    weight = (w_buf[...].astype(jnp.float32) * gain_buf[...]).T.astype(jnp.bfloat16)
+    half = weight.shape[1] // 2
+    blocks = x_buf.shape[0] // BLOCK
+    for j in range(pieces):
+        copies[j].wait()
+        x = x_buf[rows * j : rows * j + rows, :]
+        wide = x.astype(jnp.float32)
+        inverse = lax.rsqrt(jnp.mean(wide * wide, axis=1, keepdims=True) + NORM_EPS)
+        turned = (jnp.dot(x, weight, preferred_element_type=jnp.float32) * inverse).T
+        for b in range(rows // BLOCK):
+            for c in range(2):
+                place = rows // BLOCK * j + b + blocks * c
+                scr[:, place, :] = turned[half * c : half * c + half, BLOCK * b : BLOCK * b + BLOCK]
+    out_ref[...] = scr[...].astype(jnp.bfloat16)
+
+
+def project(tokens, w_in, gain):
     rows, width = tokens.shape
-    channels = weight.shape[1]
-    steps = rows // BLOCK
-    shape = (channels // 2, 2 * steps, BLOCK)
+    channels = w_in.shape[1]
+    pieces = 4
+    shape = (channels // 2, 2 * rows // BLOCK, BLOCK)
+    inputs = [
+        pltpu.with_memory_space_constraint(a, pltpu.HBM) for a in (tokens, w_in.T, gain[None])
+    ]
     return pl.pallas_call(
         project_body,
-        grid=(steps,),
-        in_specs=[
-            pl.BlockSpec((BLOCK, width), lambda s: (s, 0)),
-            pl.BlockSpec((width, channels), lambda s: (0, 0)),
+        in_specs=[pl.BlockSpec(memory_space=pltpu.HBM)] * 3,
+        out_specs=pl.BlockSpec(memory_space=pltpu.VMEM),
+        out_shape=pltpu.VMEM(shape, jnp.bfloat16),
+        scratch_shapes=[
+            pltpu.VMEM((rows, width), jnp.bfloat16),
+            pltpu.VMEM((channels, width), jnp.bfloat16),
+            pltpu.VMEM((1, width), jnp.float32),
+            pltpu.VMEM(shape, jnp.float32),
+            pltpu.SemaphoreType.DMA((pieces + 2,)),
         ],
-        out_specs=pl.BlockSpec(shape, lambda s: (0, 0, 0)),
-        out_shape=jax.ShapeDtypeStruct(shape, jnp.bfloat16),
-        scratch_shapes=[pltpu.VMEM(shape, jnp.float32)],
-        compiler_params=pltpu.CompilerParams(dimension_semantics=("arbitrary",)),
-    )(tokens, weight)
+        compiler_params=pltpu.CompilerParams(vmem_limit_bytes=24 << 20),
+    )(*inputs)
 
 
 def fft_tables(total, n_first, n_second):
@@ -99,8 +118,9 @@
     shape = (BLOCK, 8, BLOCK)
     return pl.pallas_call(
         positions_body,
-        out_shape=jax.ShapeDtypeStruct(shape, jnp.bfloat16),
+        out_shape=pltpu.VMEM(shape, jnp.bfloat16),
         scratch_shapes=[pltpu.VMEM(shape, jnp.float32)],
+        compiler_params=SMALL,
     )(arrived, *tables)
 
 
@@ -130,8 +150,9 @@
     count = arrived.shape[1] * arrived.shape[2] // 4
     return pl.pallas_call(
         channels_body,
-        out_shape=jax.ShapeDtypeStruct((count, GROUP), jnp.bfloat16),
+        out_shape=pltpu.VMEM((count, GROUP), jnp.bfloat16),
         scratch_shapes=[pltpu.VMEM(arrived.shape, jnp.float32)],
+        compiler_params=SMALL,
     )(arrived, table)
 
 
@@ -161,7 +182,8 @@
             pl.BlockSpec(memory_space=pltpu.VMEM),
             pl.BlockSpec(memory_space=pltpu.VMEM),
         ],
-        out_shape=jax.ShapeDtypeStruct((4, count, own.shape[2]), jnp.bfloat16),
+        out_shape=pltpu.VMEM((4, count, own.shape[2]), jnp.bfloat16),
+        compiler_params=SMALL,
     )(half, gathered, own, other)
 
 
@@ -170,8 +192,7 @@
     total = tokens.shape[0] * rows
     own = lax.all_gather(w_out, "k", axis=0)
     other = lax.ppermute(own, "h", [(0, 1), (1, 0)])
-    weight = (w_in.astype(jnp.float32) * norm_gain[:, None]).astype(jnp.bfloat16)
-    projected = project(tokens, weight)
+    projected = project(tokens, w_in, norm_gain)
     arrived = lax.all_to_all(projected, "row", 0, 0, tiled=True)
     spectra = positions(arrived, total)
     arrived = lax.all_to_all(spectra, ("row", "h", "k"), 0, 0, tiled=True)

time: 93 us -> 79.5 us (0.85)
  Pallas kernels: 14.7 us -> 6.53 us
  local copies, waits for them, and re-layouts: 3.36 us -> 0.72 us
  other arithmetic: 1.87 us -> 0 us
    pallas_call x3, Pallas kernels: 12 us -> 5.82 us  [the longest x1 3.6 us: project(): pl.pallas_call(project_body, in_specs=[pl.BlockSpec(memory_space=pltpu.HB...]
    pallas_call x1, Pallas kernels: 2.76 us -> 0.71 us  [output_map(): pl.pallas_call(output_body, in_specs=[pl.BlockSpec(memory_space=pltpu.SME...]
    convert_element_type x1 -> x0, other arithmetic: 1.87 us -> none  [local(): (w_in.astype(jnp.float32) * norm_gain[:, None]).astype(jnp.bfloat16)]
    unnamed x9 -> x11, local copies, waits for them, and re-layouts: 2.21 us -> 0.72 us
    convert_element_type x1 -> x0, local copies, waits for them, and re-layouts: 1.15 us -> none  [local(): w_in.astype(jnp.float32) * norm_gain[:, None]]
  transfers between devices with their start and end apart: 2 -> 2, of which waited for: 1 -> 1; matrix products, arithmetic and copies ran while one was open for 0% -> 0% of each run, Pallas kernels for 2% -> 1%
where the time goes in v2:
time: 79.5 us; the launch traced here: 79.3 us
  blocking collectives  53.5 us (67%)
  starting transfers between devices  10.3 us (13%)
  waiting for transfers between devices  8.19 us (10%)
  Pallas kernels  6.53 us (8%)
    all_to_all x1, blocking collectives, local(): arrived = lax.all_to_all(projected, 'row', 0, 0, tiled=True)  22.9 us
    all_gather x1, blocking collectives, local(): gathered = lax.all_gather(mixed, 'g', axis=0)  17.2 us
    all_to_all x1, blocking collectives, local(): output = lax.all_to_all(output, ('h', 'k'), 0, 0, tiled=True)  10.7 us
    all_to_all x1, waiting for transfers between devices, local(): arrived = lax.all_to_all(spectra, ('row', 'h', 'k'), 0, 0, tiled=True)  8.18 us
    all_to_all x1, starting transfers between devices, local(): arrived = lax.all_to_all(spectra, ('row', 'h', 'k'), 0, 0, tiled=True)  7.54 us
    pallas_call x1, Pallas kernels, project(): pl.pallas_call(project_body, in_specs=[pl.BlockSpec(memory_space=pltpu.HB...  3.6 us
    ppermute x1, starting transfers between devices, local(): other = lax.ppermute(own, 'h', [(0, 1), (1, 0)])  2.75 us
    all_gather x1, blocking collectives, local(): own = lax.all_gather(w_out, 'k', axis=0)  2.7 us
  transfers between devices with their start and end apart: 2, of which 1 were waited for; matrix products, arithmetic and copies ran while one was open for 0% of the time, Pallas kernels for 1%

profile of v2, /device:TPU:1, one launch (start us, length us, event | category | flops | bytes accessed | tf_op | source)
XLA Modules:
  0.0 79.3 jit_solution(6633038796829346203)
XLA Ops:
  0.0 0.0 copy-start.3
  0.0 0.0 copy-start.1
  0.0 0.0 copy-start.2
  0.0 0.0 copy-start
  0.0 0.0 copy-start.4
  0.0 3.6 %shard_map.82 = bf16[32,16,128]{2,1,0:T(8,128)(2,1)S(1)} custom-call(bf16[1024,2048]{1,0:T(8,128)(2,1)} %x_hbm.1, bf16[64,2048]{1,0:T(8,128)(2,1)} %bitcast.10, f32[1,2048]{1,0:T(1,128)} %bitcast.11), custom_call_target="tpu_custom_call" | custom-call | tf_op jit(solution)/shard_map/pallas_call | solution.py:56
  3.6 22.9 %all_to_all.15.x_ref = bf16[32,16,128]{2,1,0:T(8,128)(2,1)S(1)} all-to-all(bf16[32,16,128]{2,1,0:T(8,128)(2,1)S(1)} %shard_map.82), channel_id=1, replica_groups=mesh['row'=32,'g'=4,'h'=2,'k'=2] {'row'}, dimensions={0} | all-to-all | bytes 262144 | tf_op jit(solution)/shard_map/all_to_all | solution.py:196
  26.5 0.0 copy-done.3
  26.5 0.0 copy-done.1
  26.5 0.0 copy-done.2
  26.5 1.7 %shard_map.83 = bf16[128,8,128]{2,1,0:T(8,128)(2,1)} custom-call(bf16[32,16,128]{2,1,0:T(8,128)(2,1)S(1)} %all_to_all.15.x_ref, bf16[512,256]{1,0:T(8,128)(2,1)S(1)} %copy-done.2, f32[2,256,128]{2,1,0:T(8,128)S(1)} %copy-done.1, bf16[256,256]{1,0:T(8,128)(2,1)S(1)} %copy-done.3), custom_call_target="tpu_custom_call" | custom-call | tf_op jit(solution)/shard_map/pallas_call | solution.py:119
  28.2 7.5 %all-to-all-start.1 = ((bf16[128,8,128]{2,1,0:T(8,128)(2,1)}), bf16[128,8,128]{2,1,0:T(8,128)(2,1)S(1)}, u32[]{:S(2)}, u32[]{:S(2)}) async-start(bf16[128,8,128]{2,1,0:T(8,128)(2,1)} %shard_map.83), calls=%async_computation.1 | async-start | bytes 524288 | tf_op jit(solution)/shard_map/all_to_all | solution.py:198
  35.7 0.0 copy-done.4
  35.7 2.7 %all-gather.1 = bf16[2048,128]{1,0:T(8,128)(2,1)S(1)} all-gather(bf16[1024,128]{1,0:T(8,128)(2,1)S(1)} %copy-done.4), channel_id=3, replica_groups=mesh['row'=32,'g'=4,'h'=2,'k'=2] {'k'}, dimensions={0}, use_global_device_ids=true | all-gather | bytes 786432 | tf_op jit(solution)/shard_map/all_gather | solution.py:193
  38.4 2.7 %collective-permute-start = (bf16[2,1024,128]{2,1,0:T(8,128)(2,1)S(1)}, bf16[2,1024,128]{2,1,0:T(8,128)(2,1)S(1)}, u32[]{:S(2)}, u32[]{:S(2)}) collective-permute-start(bf16[2,1024,128]{2,1,0:T(8,128)(2,1)S(1)} %bitcast.7), channel_id=1, source_target_pairs={{0,2},{2,0},{1,3},{3,1},{4,6},{6,4},{5,7},{7,5},{8,10},{10,8},{9,1... | collective-permute-start | bytes 1572872 | tf_op jit(solution)/shard_map/ppermute | solution.py:194
  41.2 8.2 %all-to-all-done.1.x_ref = bf16[128,8,128]{2,1,0:T(8,128)(2,1)S(1)} async-done(((bf16[128,8,128]{2,1,0:T(8,128)(2,1)}), bf16[128,8,128]{2,1,0:T(8,128)(2,1)S(1)}, u32[]{:S(2)}, u32[]{:S(2)}) %all-to-all-start.1) | async-done | bytes 262176 | tf_op jit(solution)/shard_map/all_to_all | solution.py:198
  49.4 0.0 copy-done
  49.4 0.5 shard_map.84
  49.9 17.2 %all-gather = bf16[1024,256]{1,0:T(8,128)(2,1)S(1)} all-gather(bf16[256,256]{1,0:T(8,128)(2,1)S(1)} %shard_map.84), channel_id=2, replica_groups=mesh['row'=32,'g'=4,'h'=2,'k'=2] {'g'}, dimensions={0}, use_global_device_ids=true | all-gather | bytes 655360 | tf_op jit(solution)/shard_map/all_gather | solution.py:200
  67.1 0.0 collective-permute-done.other_ref
  67.1 0.7 shard_map.85
  67.8 10.7 %all_to_all.16 = bf16[4,256,128]{2,1,0:T(8,128)(2,1)S(1)} all-to-all(bf16[4,256,128]{2,1,0:T(8,128)(2,1)S(1)} %shard_map.85), channel_id=1, replica_groups=mesh['row'=32,'g'=4,'h'=2,'k'=2] {'h','k'}, dimensions={0} | all-to-all | bytes 524288 | tf_op jit(solution)/shard_map/all_to_all | solution.py:203
  78.6 0.7 copy.10
Async XLA Ops:
  0.0 26.5 %copy-start.3 = (bf16[256,256]{1,0:T(8,128)(2,1)S(1)}, bf16[256,256]{1,0:T(8,128)(2,1)}, u32[]{:S(2)}) copy-start(bf16[256,256]{1,0:T(8,128)(2,1)} %constant.14.clone.two_ref) | copy-start | bytes 393220
  0.0 26.5 %copy-start.1 = (f32[2,256,128]{2,1,0:T(8,128)S(1)}, f32[2,256,128]{2,1,0:T(8,128)}, u32[]{:S(2)}) copy-start(f32[2,256,128]{2,1,0:T(8,128)} %constant.13.clone.turn_ref) | copy-start | bytes 786436
  0.0 26.5 %copy-start.2 = (bf16[512,256]{1,0:T(8,128)(2,1)S(1)}, bf16[512,256]{1,0:T(8,128)(2,1)}, u32[]{:S(2)}) copy-start(bf16[512,256]{1,0:T(8,128)(2,1)} %constant.12.clone.one_ref) | copy-start | bytes 786436
  0.0 49.4 %copy-start = (bf16[256,512]{1,0:T(8,128)(2,1)S(1)}, bf16[256,512]{1,0:T(8,128)(2,1)}, u32[]{:S(2)}) copy-start(bf16[256,512]{1,0:T(8,128)(2,1)} %constant.15.clone.table_ref) | copy-start | bytes 786436
  0.0 35.7 %copy-start.4 = (bf16[1024,128]{1,0:T(8,128)(2,1)S(1)}, bf16[1024,128]{1,0:T(8,128)(2,1)}, u32[]{:S(2)}) copy-start(bf16[1024,128]{1,0:T(8,128)(2,1)} %param.11) | copy-start | bytes 786436
  28.2 21.2 %all-to-all-start.1 = ((bf16[128,8,128]{2,1,0:T(8,128)(2,1)}), bf16[128,8,128]{2,1,0:T(8,128)(2,1)S(1)}, u32[]{:S(2)}, u32[]{:S(2)}) async-start(bf16[128,8,128]{2,1,0:T(8,128)(2,1)} %shard_map.83), calls=%async_computation.1 | async-start | bytes 524288 | tf_op jit(solution)/shard_map/all_to_all | solution.py:198
  38.4 28.7 %collective-permute-start = (bf16[2,1024,128]{2,1,0:T(8,128)(2,1)S(1)}, bf16[2,1024,128]{2,1,0:T(8,128)(2,1)S(1)}, u32[]{:S(2)}, u32[]{:S(2)}) collective-permute-start(bf16[2,1024,128]{2,1,0:T(8,128)(2,1)S(1)} %bitcast.7), channel_id=1, source_target_pairs={{0,2},{2,0},{1,3},{3,1},{4,6},{6,4},{5,7},{7,5},{8,10},{10,8},{9,1... | collective-permute-start | bytes 1572872 | tf_op jit(solution)/shard_map/ppermute | solution.py:194

commit v3 on v2

--- a/solution.py
+++ b/solution.py
@@ -12,6 +12,7 @@
 GROUP = 256
 NORM_EPS = 1e-06
 BLOCK = 128
+AHEAD = 3
 SMALL = pltpu.CompilerParams(vmem_limit_bytes=16 << 20)
 
 
@@ -26,22 +27,35 @@
     for j in range(pieces):
         span = pl.ds(rows * j, rows)
         copies.append(pltpu.make_async_copy(x_hbm.at[span], x_buf.at[span], sems.at[j]))
+    for j in range(AHEAD):
         copies[j].start()
     weights.wait()
     gains.wait()
     weight = (w_buf[...].astype(jnp.float32) * gain_buf[...]).T.astype(jnp.bfloat16)
     half = weight.shape[1] // 2
     blocks = x_buf.shape[0] // BLOCK
-    for j in range(pieces):
-        copies[j].wait()
-        x = x_buf[rows * j : rows * j + rows, :]
-        wide = x.astype(jnp.float32)
-        inverse = lax.rsqrt(jnp.mean(wide * wide, axis=1, keepdims=True) + NORM_EPS)
-        turned = (jnp.dot(x, weight, preferred_element_type=jnp.float32) * inverse).T
+
+
+    def finish(j, part, square):
+        turned = (part * lax.rsqrt(square + NORM_EPS)).T
         for b in range(rows // BLOCK):
             for c in range(2):
                 place = rows // BLOCK * j + b + blocks * c
                 scr[:, place, :] = turned[half * c : half * c + half, BLOCK * b : BLOCK * b + BLOCK]
+
+    waiting = None
+    for j in range(pieces):
+        copies[j].wait()
+        if j + AHEAD < pieces:
+            copies[j + AHEAD].start()
+        x = x_buf[rows * j : rows * j + rows, :]
+        wide = x.astype(jnp.float32)
+        square = jnp.mean(wide * wide, axis=1, keepdims=True)
+        part = jnp.dot(x, weight, preferred_element_type=jnp.float32)
+        if waiting is not None:
+            finish(*waiting)
+        waiting = (j, part, square)
+    finish(*waiting)
     out_ref[...] = scr[...].astype(jnp.bfloat16)
 
 
@@ -156,23 +170,25 @@
     )(arrived, table)
 
 
-def output_body(half_ref, spec_ref, own_ref, other_ref, out_ref):
-    half = half_ref[0]
+def output_body(place_ref, spec_ref, own_ref, other_ref, out_ref):
+    half, core = place_ref[0], place_ref[1]
     groups = spec_ref.shape[0]
+    spans = [
+        pl.ds(pl.multiple_of(GROUP * jnp.where(core == 0, g, (groups - g) % groups), GROUP), GROUP)
+        for g in range(groups)
+    ]
     for k in range(2):
         for ref, place in ((own_ref, 2 * half + k), (other_ref, 2 * (1 - half) + k)):
             total = None
             for g in range(groups):
                 part = jnp.dot(
-                    spec_ref[g],
-                    ref[k, GROUP * g : GROUP * g + GROUP, :],
-                    preferred_element_type=jnp.float32,
+                    spec_ref[g], ref[k, spans[g], :], preferred_element_type=jnp.float32
                 )
                 total = part if total is None else total + part
             out_ref[pl.ds(place, 1)] = total.astype(jnp.bfloat16)[None]
 
 
-def output_map(half, gathered, own, other):
+def output_map(place, gathered, own, other):
     count = gathered.shape[1]
     return pl.pallas_call(
         output_body,
@@ -184,7 +200,7 @@
         ],
         out_shape=pltpu.VMEM((4, count, own.shape[2]), jnp.bfloat16),
         compiler_params=SMALL,
-    )(half, gathered, own, other)
+    )(place, gathered, own, other)
 
 
 def local(tokens, norm_gain, w_in, w_out):
@@ -197,9 +213,14 @@
     spectra = positions(arrived, total)
     arrived = lax.all_to_all(spectra, ("row", "h", "k"), 0, 0, tiled=True)
     mixed = channel_mix(arrived, channel_table(rows, 4))
-    gathered = lax.all_gather(mixed, "g", axis=0)
-    half = lax.axis_index("h").astype(jnp.int32).reshape(1)
-    output = output_map(half, gathered, own, other)
+    far = [
+        [4 * (g if k == 0 else -g % 4) + 2 * h + k for g in range(4)]
+        for h in range(2)
+        for k in range(2)
+    ]
+    gathered = lax.all_gather(mixed, ("g", "h", "k"), axis=0, axis_index_groups=far)
+    place = jnp.stack([lax.axis_index("h"), lax.axis_index("k")]).astype(jnp.int32)
+    output = output_map(place, gathered, own, other)
     output = lax.all_to_all(output, ("h", "k"), 0, 0, tiled=True)
     return output.reshape(tokens.shape[0], w_out.shape[1])
 

time: 79.5 us -> 79.9 us (level)
  no operation moved by 1% of the time
where the time goes in v3:
time: 79.9 us; the launch traced here: 79.6 us
  blocking collectives  53.4 us (67%)
  starting transfers between devices  10.3 us (13%)
  waiting for transfers between devices  8.11 us (10%)
  Pallas kernels  6.89 us (9%)
    all_to_all x1, blocking collectives, local(): arrived = lax.all_to_all(projected, 'row', 0, 0, tiled=True)  22.9 us
    all_gather x1, blocking collectives, local(): lax.all_gather(mixed, ('g', 'h', 'k'), axis=0, axis_index_groups=far)  17.1 us
    all_to_all x1, blocking collectives, local(): output = lax.all_to_all(output, ('h', 'k'), 0, 0, tiled=True)  10.8 us
    all_to_all x1, waiting for transfers between devices, local(): arrived = lax.all_to_all(spectra, ('row', 'h', 'k'), 0, 0, tiled=True)  8.11 us
    all_to_all x1, starting transfers between devices, local(): arrived = lax.all_to_all(spectra, ('row', 'h', 'k'), 0, 0, tiled=True)  7.54 us
    pallas_call x1, Pallas kernels, project(): pl.pallas_call(project_body, in_specs=[pl.BlockSpec(memory_space=pltpu.HB...  3.42 us
    ppermute x1, starting transfers between devices, local(): other = lax.ppermute(own, 'h', [(0, 1), (1, 0)])  2.75 us
    all_gather x1, blocking collectives, local(): own = lax.all_gather(w_out, 'k', axis=0)  2.7 us
  transfers between devices with their start and end apart: 2, of which 1 were waited for; matrix products, arithmetic and copies ran while one was open for 0% of the time, Pallas kernels for 1%

profile of v3, /device:TPU:1, one launch (start us, length us, event | category | flops | bytes accessed | tf_op | source)
XLA Modules:
  0.0 79.6 jit_solution(15102624971674468877)
XLA Ops:
  0.0 0.0 copy-start.3
  0.0 0.0 copy-start.1
  0.0 0.0 copy-start.2
  0.0 0.0 copy-start
  0.0 0.0 copy-start.4
  0.0 3.4 %shard_map.82 = bf16[32,16,128]{2,1,0:T(8,128)(2,1)S(1)} custom-call(bf16[1024,2048]{1,0:T(8,128)(2,1)} %x_hbm.1, bf16[64,2048]{1,0:T(8,128)(2,1)} %bitcast.11, f32[1,2048]{1,0:T(1,128)} %bitcast.12), custom_call_target="tpu_custom_call" | custom-call | tf_op jit(solution)/shard_map/pallas_call | solution.py:70
  3.5 22.9 %all_to_all.15.x_ref = bf16[32,16,128]{2,1,0:T(8,128)(2,1)S(1)} all-to-all(bf16[32,16,128]{2,1,0:T(8,128)(2,1)S(1)} %shard_map.82), channel_id=1, replica_groups=mesh['row'=32,'g'=4,'h'=2,'k'=2] {'row'}, dimensions={0} | all-to-all | bytes 262144 | tf_op jit(solution)/shard_map/all_to_all | solution.py:212
  26.3 0.0 copy-done.3
  26.3 0.0 copy-done.1
  26.3 0.0 copy-done.2
  26.3 1.7 %shard_map.83 = bf16[128,8,128]{2,1,0:T(8,128)(2,1)} custom-call(bf16[32,16,128]{2,1,0:T(8,128)(2,1)S(1)} %all_to_all.15.x_ref, bf16[512,256]{1,0:T(8,128)(2,1)S(1)} %copy-done.2, f32[2,256,128]{2,1,0:T(8,128)S(1)} %copy-done.1, bf16[256,256]{1,0:T(8,128)(2,1)S(1)} %copy-done.3), custom_call_target="tpu_custom_call" | custom-call | tf_op jit(solution)/shard_map/pallas_call | solution.py:133
  28.0 7.5 %all-to-all-start.1 = ((bf16[128,8,128]{2,1,0:T(8,128)(2,1)}), bf16[128,8,128]{2,1,0:T(8,128)(2,1)S(1)}, u32[]{:S(2)}, u32[]{:S(2)}) async-start(bf16[128,8,128]{2,1,0:T(8,128)(2,1)} %shard_map.83), calls=%async_computation.1 | async-start | bytes 524288 | tf_op jit(solution)/shard_map/all_to_all | solution.py:214
  35.6 0.0 copy-done.4
  35.6 2.7 %all-gather.1 = bf16[2048,128]{1,0:T(8,128)(2,1)S(1)} all-gather(bf16[1024,128]{1,0:T(8,128)(2,1)S(1)} %copy-done.4), channel_id=3, replica_groups=mesh['row'=32,'g'=4,'h'=2,'k'=2] {'k'}, dimensions={0}, use_global_device_ids=true | all-gather | bytes 786432 | tf_op jit(solution)/shard_map/all_gather | solution.py:209
  38.3 2.7 %collective-permute-start = (bf16[2,1024,128]{2,1,0:T(8,128)(2,1)S(1)}, bf16[2,1024,128]{2,1,0:T(8,128)(2,1)S(1)}, u32[]{:S(2)}, u32[]{:S(2)}) collective-permute-start(bf16[2,1024,128]{2,1,0:T(8,128)(2,1)S(1)} %bitcast.8), channel_id=1, source_target_pairs={{0,2},{2,0},{1,3},{3,1},{4,6},{6,4},{5,7},{7,5},{8,10},{10,8},{9,1... | collective-permute-start | bytes 1572872 | tf_op jit(solution)/shard_map/ppermute | solution.py:210
  41.0 0.1 pad_add_fusion.place_ref
  41.1 8.1 %all-to-all-done.1.x_ref = bf16[128,8,128]{2,1,0:T(8,128)(2,1)S(1)} async-done(((bf16[128,8,128]{2,1,0:T(8,128)(2,1)}), bf16[128,8,128]{2,1,0:T(8,128)(2,1)S(1)}, u32[]{:S(2)}, u32[]{:S(2)}) %all-to-all-start.1) | async-done | bytes 262176 | tf_op jit(solution)/shard_map/all_to_all | solution.py:214
  49.2 0.0 copy-done
  49.2 0.5 shard_map.84
  49.8 17.1 %all-gather = bf16[1024,256]{1,0:T(8,128)(2,1)S(1)} all-gather(bf16[256,256]{1,0:T(8,128)(2,1)S(1)} %shard_map.84), channel_id=2, replica_groups={{0,4,8,12},{1,13,9,5},{2,6,10,14},{3,15,11,7},{16,20,24,28},{17,29,25,2..., dimensions={0}, use_global_device_ids=true | all-gather | bytes 655360 | tf_op jit(solution)/shard_map/all_gather | solution.py:221
  66.9 0.0 collective-permute-done.other_ref
  66.9 1.3 %shard_map.85 = bf16[4,256,128]{2,1,0:T(8,128)(2,1)S(1)} custom-call(s32[2]{0:T(128)S(1)} %pad_add_fusion.place_ref, bf16[4,256,256]{2,1,0:T(8,128)(2,1)S(1)} %bitcast.7, bf16[2,1024,128]{2,1,0:T(8,128)(2,1)S(1)} %bitcast.9, bf16[2,1024,128]{2,1,0:T(8,128)(2,1)S(1)} %collective-permute-done.other_ref), custom_call_target="tpu_custom_call" | custom-call | tf_op jit(solution)/shard_map/pallas_call | solution.py:193
  68.1 10.8 %all_to_all.16 = bf16[4,256,128]{2,1,0:T(8,128)(2,1)S(1)} all-to-all(bf16[4,256,128]{2,1,0:T(8,128)(2,1)S(1)} %shard_map.85), channel_id=1, replica_groups=mesh['row'=32,'g'=4,'h'=2,'k'=2] {'h','k'}, dimensions={0} | all-to-all | bytes 524288 | tf_op jit(solution)/shard_map/all_to_all | solution.py:224
  78.9 0.7 copy.10
Async XLA Ops:
  0.0 26.3 %copy-start.3 = (bf16[256,256]{1,0:T(8,128)(2,1)S(1)}, bf16[256,256]{1,0:T(8,128)(2,1)}, u32[]{:S(2)}) copy-start(bf16[256,256]{1,0:T(8,128)(2,1)} %constant.16.clone.two_ref) | copy-start | bytes 393220
  0.0 26.3 %copy-start.1 = (f32[2,256,128]{2,1,0:T(8,128)S(1)}, f32[2,256,128]{2,1,0:T(8,128)}, u32[]{:S(2)}) copy-start(f32[2,256,128]{2,1,0:T(8,128)} %constant.15.clone.turn_ref) | copy-start | bytes 786436
  0.0 26.3 %copy-start.2 = (bf16[512,256]{1,0:T(8,128)(2,1)S(1)}, bf16[512,256]{1,0:T(8,128)(2,1)}, u32[]{:S(2)}) copy-start(bf16[512,256]{1,0:T(8,128)(2,1)} %constant.14.clone.one_ref) | copy-start | bytes 786436
  0.0 49.2 %copy-start = (bf16[256,512]{1,0:T(8,128)(2,1)S(1)}, bf16[256,512]{1,0:T(8,128)(2,1)}, u32[]{:S(2)}) copy-start(bf16[256,512]{1,0:T(8,128)(2,1)} %constant.17.clone.table_ref) | copy-start | bytes 786436
  0.0 35.5 %copy-start.4 = (bf16[1024,128]{1,0:T(8,128)(2,1)S(1)}, bf16[1024,128]{1,0:T(8,128)(2,1)}, u32[]{:S(2)}) copy-start(bf16[1024,128]{1,0:T(8,128)(2,1)} %param.11) | copy-start | bytes 786436
  28.0 21.2 %all-to-all-start.1 = ((bf16[128,8,128]{2,1,0:T(8,128)(2,1)}), bf16[128,8,128]{2,1,0:T(8,128)(2,1)S(1)}, u32[]{:S(2)}, u32[]{:S(2)}) async-start(bf16[128,8,128]{2,1,0:T(8,128)(2,1)} %shard_map.83), calls=%async_computation.1 | async-start | bytes 524288 | tf_op jit(solution)/shard_map/all_to_all | solution.py:214
  38.3 28.6 %collective-permute-start = (bf16[2,1024,128]{2,1,0:T(8,128)(2,1)S(1)}, bf16[2,1024,128]{2,1,0:T(8,128)(2,1)S(1)}, u32[]{:S(2)}, u32[]{:S(2)}) collective-permute-start(bf16[2,1024,128]{2,1,0:T(8,128)(2,1)S(1)} %bitcast.8), channel_id=1, source_target_pairs={{0,2},{2,0},{1,3},{3,1},{4,6},{6,4},{5,7},{7,5},{8,10},{10,8},{9,1... | collective-permute-start | bytes 1572872 | tf_op jit(solution)/shard_map/ppermute | solution.py:210

commit v4 on v2

--- a/solution.py
+++ b/solution.py
@@ -12,6 +12,7 @@
 GROUP = 256
 NORM_EPS = 1e-06
 BLOCK = 128
+AHEAD = 3
 SMALL = pltpu.CompilerParams(vmem_limit_bytes=16 << 20)
 
 
@@ -26,22 +27,35 @@
     for j in range(pieces):
         span = pl.ds(rows * j, rows)
         copies.append(pltpu.make_async_copy(x_hbm.at[span], x_buf.at[span], sems.at[j]))
+    for j in range(AHEAD):
         copies[j].start()
     weights.wait()
     gains.wait()
     weight = (w_buf[...].astype(jnp.float32) * gain_buf[...]).T.astype(jnp.bfloat16)
     half = weight.shape[1] // 2
     blocks = x_buf.shape[0] // BLOCK
-    for j in range(pieces):
-        copies[j].wait()
-        x = x_buf[rows * j : rows * j + rows, :]
-        wide = x.astype(jnp.float32)
-        inverse = lax.rsqrt(jnp.mean(wide * wide, axis=1, keepdims=True) + NORM_EPS)
-        turned = (jnp.dot(x, weight, preferred_element_type=jnp.float32) * inverse).T
+
+
+    def finish(j, part, square):
+        turned = (part * lax.rsqrt(square + NORM_EPS)).T
         for b in range(rows // BLOCK):
             for c in range(2):
                 place = rows // BLOCK * j + b + blocks * c
                 scr[:, place, :] = turned[half * c : half * c + half, BLOCK * b : BLOCK * b + BLOCK]
+
+    waiting = None
+    for j in range(pieces):
+        copies[j].wait()
+        if j + AHEAD < pieces:
+            copies[j + AHEAD].start()
+        x = x_buf[rows * j : rows * j + rows, :]
+        wide = x.astype(jnp.float32)
+        square = jnp.mean(wide * wide, axis=1, keepdims=True)
+        part = jnp.dot(x, weight, preferred_element_type=jnp.float32)
+        if waiting is not None:
+            finish(*waiting)
+        waiting = (j, part, square)
+    finish(*waiting)
     out_ref[...] = scr[...].astype(jnp.bfloat16)
 
 
@@ -143,14 +157,14 @@
     ]
     data = jnp.concatenate(rows, 0)
     spectrum = jnp.dot(table_ref[...], data, preferred_element_type=jnp.float32)
-    out_ref[...] = spectrum.T.astype(jnp.bfloat16)
-
-
-def channel_mix(arrived, table):
+    out_ref[...] = jnp.broadcast_to(spectrum.T.astype(jnp.bfloat16)[None], out_ref.shape)
+
+
+def channel_mix(arrived, table, copies):
     count = arrived.shape[1] * arrived.shape[2] // 4
     return pl.pallas_call(
         channels_body,
-        out_shape=pltpu.VMEM((count, GROUP), jnp.bfloat16),
+        out_shape=pltpu.VMEM((copies, count, GROUP), jnp.bfloat16),
         scratch_shapes=[pltpu.VMEM(arrived.shape, jnp.float32)],
         compiler_params=SMALL,
     )(arrived, table)
@@ -196,8 +210,8 @@
     arrived = lax.all_to_all(projected, "row", 0, 0, tiled=True)
     spectra = positions(arrived, total)
     arrived = lax.all_to_all(spectra, ("row", "h", "k"), 0, 0, tiled=True)
-    mixed = channel_mix(arrived, channel_table(rows, 4))
-    gathered = lax.all_gather(mixed, "g", axis=0)
+    mixed = channel_mix(arrived, channel_table(rows, 4), 4)
+    gathered = lax.all_to_all(mixed, "g", 0, 0, tiled=True)
     half = lax.axis_index("h").astype(jnp.int32).reshape(1)
     output = output_map(half, gathered, own, other)
     output = lax.all_to_all(output, ("h", "k"), 0, 0, tiled=True)

time: 79.5 us -> 90.3 us (1.14)
  waiting for transfers between devices: 8.19 us -> 18.7 us
  blocking collectives: 53.5 us -> 54.9 us
  starting transfers between devices: 10.3 us -> 9.12 us
    all_to_all x0 -> x1, blocking collectives: none -> 21 us  [local(): arrived = lax.all_to_all(spectra, ('row', 'h', 'k'), 0, 0, tiled=True)]
    ppermute x1, waiting for transfers between devices: 0.01 us -> 18.7 us  [local(): other = lax.ppermute(own, 'h', [(0, 1), (1, 0)])]
    all_gather x1 -> x0, blocking collectives: 17.2 us -> none  [local(): gathered = lax.all_gather(mixed, 'g', axis=0)]
    all_to_all x1, waiting for transfers between devices: 8.18 us -> 0.01 us  [local(): gathered = lax.all_to_all(mixed, 'g', 0, 0, tiled=True)]
    all_to_all x1, blocking collectives: 10.7 us -> 8.6 us  [local(): output = lax.all_to_all(output, ('h', 'k'), 0, 0, tiled=True)]
    all_to_all x1, starting transfers between devices: 7.54 us -> 6.18 us  [local(): gathered = lax.all_to_all(mixed, 'g', 0, 0, tiled=True)]
  transfers between devices with their start and end apart: 2 -> 2, of which waited for: 1 -> 1; matrix products, arithmetic and copies ran while one was open for 0% -> 0% of each run, Pallas kernels for 1% -> 0%
where the time goes in v4:
time: 90.3 us; the launch traced here: 90 us
  blocking collectives  54.9 us (61%)
  waiting for transfers between devices  18.7 us (21%)
  starting transfers between devices  9.12 us (10%)
  Pallas kernels  6.44 us (7%)
    all_to_all x1, blocking collectives, local(): arrived = lax.all_to_all(projected, 'row', 0, 0, tiled=True)  22.9 us
    all_to_all x1, blocking collectives, local(): arrived = lax.all_to_all(spectra, ('row', 'h', 'k'), 0, 0, tiled=True)  21 us
    ppermute x1, waiting for transfers between devices, local(): other = lax.ppermute(own, 'h', [(0, 1), (1, 0)])  18.7 us
    all_to_all x1, blocking collectives, local(): output = lax.all_to_all(output, ('h', 'k'), 0, 0, tiled=True)  8.6 us
    all_to_all x1, starting transfers between devices, local(): gathered = lax.all_to_all(mixed, 'g', 0, 0, tiled=True)  6.18 us
    pallas_call x1, Pallas kernels, project(): pl.pallas_call(project_body, in_specs=[pl.BlockSpec(memory_space=pltpu.HB...  3.42 us
    ppermute x1, starting transfers between devices, local(): other = lax.ppermute(own, 'h', [(0, 1), (1, 0)])  2.94 us
    all_gather x1, blocking collectives, local(): own = lax.all_gather(w_out, 'k', axis=0)  2.47 us
  transfers between devices with their start and end apart: 2, of which 1 were waited for; matrix products, arithmetic and copies ran while one was open for 0% of the time, Pallas kernels for 0%

profile of v4, /device:TPU:1, one launch (start us, length us, event | category | flops | bytes accessed | tf_op | source)
XLA Modules:
  0.0 90.0 jit_solution(3402859052772625544)
XLA Ops:
  0.0 0.0 copy-start.3
  0.0 0.0 copy-start.1
  0.0 0.0 copy-start.2
  0.0 0.0 copy-start
  0.0 0.0 copy-start.4
  0.0 3.4 %shard_map.82 = bf16[32,16,128]{2,1,0:T(8,128)(2,1)S(1)} custom-call(bf16[1024,2048]{1,0:T(8,128)(2,1)} %x_hbm.1, bf16[64,2048]{1,0:T(8,128)(2,1)} %bitcast.8, f32[1,2048]{1,0:T(1,128)} %bitcast.9), custom_call_target="tpu_custom_call" | custom-call | tf_op jit(solution)/shard_map/pallas_call | solution.py:70
  3.5 22.9 %all_to_all.20.x_ref = bf16[32,16,128]{2,1,0:T(8,128)(2,1)S(1)} all-to-all(bf16[32,16,128]{2,1,0:T(8,128)(2,1)S(1)} %shard_map.82), channel_id=1, replica_groups=mesh['row'=32,'g'=4,'h'=2,'k'=2] {'row'}, dimensions={0} | all-to-all | bytes 262144 | tf_op jit(solution)/shard_map/all_to_all | solution.py:210
  26.3 0.0 copy-done.3
  26.3 0.0 copy-done.1
  26.3 0.0 copy-done.2
  26.3 1.0 %shard_map.83 = bf16[128,8,128]{2,1,0:T(8,128)(2,1)S(1)} custom-call(bf16[32,16,128]{2,1,0:T(8,128)(2,1)S(1)} %all_to_all.20.x_ref, bf16[512,256]{1,0:T(8,128)(2,1)S(1)} %copy-done.2, f32[2,256,128]{2,1,0:T(8,128)S(1)} %copy-done.1, bf16[256,256]{1,0:T(8,128)(2,1)S(1)} %copy-done.3), custom_call_target="tpu_custom_call" | custom-call | tf_op jit(solution)/shard_map/pallas_call | solution.py:133
  27.3 21.0 %all_to_all.21.x_ref = bf16[128,8,128]{2,1,0:T(8,128)(2,1)S(1)} all-to-all(bf16[128,8,128]{2,1,0:T(8,128)(2,1)S(1)} %shard_map.83), channel_id=1, replica_groups=mesh['row'=32,'g'=4,'h'=2,'k'=2] {'row','h','k'}, dimensions={0} | all-to-all | bytes 524288 | tf_op jit(solution)/shard_map/all_to_all | solution.py:212
  48.3 0.0 copy-done
  48.3 1.4 %shard_map.84 = bf16[4,256,256]{2,1,0:T(8,128)(2,1)} custom-call(bf16[128,8,128]{2,1,0:T(8,128)(2,1)S(1)} %all_to_all.21.x_ref, bf16[256,512]{1,0:T(8,128)(2,1)S(1)} %copy-done), custom_call_target="tpu_custom_call" | custom-call | tf_op jit(solution)/shard_map/pallas_call | solution.py:165
  49.7 6.2 %all-to-all-start.2 = ((bf16[4,256,256]{2,1,0:T(8,128)(2,1)}), bf16[4,256,256]{2,1,0:T(8,128)(2,1)S(1)}, u32[]{:S(2)}, u32[]{:S(2)}) async-start(bf16[4,256,256]{2,1,0:T(8,128)(2,1)} %shard_map.84), calls=%async_computation.2 | async-start | bytes 1048576 | tf_op jit(solution)/shard_map/all_to_all | solution.py:214
  55.8 0.0 copy-done.4
  55.8 2.5 %all-gather = bf16[2048,128]{1,0:T(8,128)(2,1)S(1)} all-gather(bf16[1024,128]{1,0:T(8,128)(2,1)S(1)} %copy-done.4), channel_id=2, replica_groups=mesh['row'=32,'g'=4,'h'=2,'k'=2] {'k'}, dimensions={0}, use_global_device_ids=true | all-gather | bytes 786432 | tf_op jit(solution)/shard_map/all_gather | solution.py:207
  58.3 2.9 %collective-permute-start = (bf16[2,1024,128]{2,1,0:T(8,128)(2,1)S(1)}, bf16[2,1024,128]{2,1,0:T(8,128)(2,1)S(1)}, u32[]{:S(2)}, u32[]{:S(2)}) collective-permute-start(bf16[2,1024,128]{2,1,0:T(8,128)(2,1)S(1)} %bitcast.5), channel_id=1, source_target_pairs={{0,2},{2,0},{1,3},{3,1},{4,6},{6,4},{5,7},{7,5},{8,10},{10,8},{9,1... | collective-permute-start | bytes 1572872 | tf_op jit(solution)/shard_map/ppermute | solution.py:208
  61.3 18.7 %collective-permute-done.other_ref = bf16[2,1024,128]{2,1,0:T(8,128)(2,1)S(1)} collective-permute-done((bf16[2,1024,128]{2,1,0:T(8,128)(2,1)S(1)}, bf16[2,1024,128]{2,1,0:T(8,128)(2,1)S(1)}, u32[]{:S(2)}, u32[]{:S(2)}) %collective-permute-start) | collective-permute-done | bytes 524320 | tf_op jit(solution)/shard_map/ppermute | solution.py:208
  80.0 0.0 all-to-all-done.2.spec_ref
  80.0 0.7 shard_map.85
  80.7 8.6 %all_to_all.22 = bf16[4,256,128]{2,1,0:T(8,128)(2,1)S(1)} all-to-all(bf16[4,256,128]{2,1,0:T(8,128)(2,1)S(1)} %shard_map.85), channel_id=1, replica_groups=mesh['row'=32,'g'=4,'h'=2,'k'=2] {'h','k'}, dimensions={0} | all-to-all | bytes 524288 | tf_op jit(solution)/shard_map/all_to_all | solution.py:217
  89.3 0.7 copy.10
Async XLA Ops:
  0.0 26.3 %copy-start.3 = (bf16[256,256]{1,0:T(8,128)(2,1)S(1)}, bf16[256,256]{1,0:T(8,128)(2,1)}, u32[]{:S(2)}) copy-start(bf16[256,256]{1,0:T(8,128)(2,1)} %constant.14.clone.two_ref) | copy-start | bytes 393220
  0.0 26.3 %copy-start.1 = (f32[2,256,128]{2,1,0:T(8,128)S(1)}, f32[2,256,128]{2,1,0:T(8,128)}, u32[]{:S(2)}) copy-start(f32[2,256,128]{2,1,0:T(8,128)} %constant.13.clone.turn_ref) | copy-start | bytes 786436
  0.0 26.3 %copy-start.2 = (bf16[512,256]{1,0:T(8,128)(2,1)S(1)}, bf16[512,256]{1,0:T(8,128)(2,1)}, u32[]{:S(2)}) copy-start(bf16[512,256]{1,0:T(8,128)(2,1)} %constant.12.clone.one_ref) | copy-start | bytes 786436
  0.0 48.3 %copy-start = (bf16[256,512]{1,0:T(8,128)(2,1)S(1)}, bf16[256,512]{1,0:T(8,128)(2,1)}, u32[]{:S(2)}) copy-start(bf16[256,512]{1,0:T(8,128)(2,1)} %constant.15.clone.table_ref) | copy-start | bytes 786436
  0.0 55.8 %copy-start.4 = (bf16[1024,128]{1,0:T(8,128)(2,1)S(1)}, bf16[1024,128]{1,0:T(8,128)(2,1)}, u32[]{:S(2)}) copy-start(bf16[1024,128]{1,0:T(8,128)(2,1)} %param.11) | copy-start | bytes 786436
  49.7 30.3 %all-to-all-start.2 = ((bf16[4,256,256]{2,1,0:T(8,128)(2,1)}), bf16[4,256,256]{2,1,0:T(8,128)(2,1)S(1)}, u32[]{:S(2)}, u32[]{:S(2)}) async-start(bf16[4,256,256]{2,1,0:T(8,128)(2,1)} %shard_map.84), calls=%async_computation.2 | async-start | bytes 1048576 | tf_op jit(solution)/shard_map/all_to_all | solution.py:214
  58.3 21.7 %collective-permute-start = (bf16[2,1024,128]{2,1,0:T(8,128)(2,1)S(1)}, bf16[2,1024,128]{2,1,0:T(8,128)(2,1)S(1)}, u32[]{:S(2)}, u32[]{:S(2)}) collective-permute-start(bf16[2,1024,128]{2,1,0:T(8,128)(2,1)S(1)} %bitcast.5), channel_id=1, source_target_pairs={{0,2},{2,0},{1,3},{3,1},{4,6},{6,4},{5,7},{7,5},{8,10},{10,8},{9,1... | collective-permute-start | bytes 1572872 | tf_op jit(solution)/shard_map/ppermute | solution.py:208

commit v5 on v4

--- a/solution.py
+++ b/solution.py
@@ -210,9 +210,10 @@
     arrived = lax.all_to_all(projected, "row", 0, 0, tiled=True)
     spectra = positions(arrived, total)
     arrived = lax.all_to_all(spectra, ("row", "h", "k"), 0, 0, tiled=True)
+    half = lax.axis_index("h").astype(jnp.int32).reshape(1)
+    arrived, own, other, half = lax.optimization_barrier((arrived, own, other, half))
     mixed = channel_mix(arrived, channel_table(rows, 4), 4)
     gathered = lax.all_to_all(mixed, "g", 0, 0, tiled=True)
-    half = lax.axis_index("h").astype(jnp.int32).reshape(1)
     output = output_map(half, gathered, own, other)
     output = lax.all_to_all(output, ("h", "k"), 0, 0, tiled=True)
     return output.reshape(tokens.shape[0], w_out.shape[1])

time: 90.3 us -> 84.5 us (0.936)
  blocking collectives: 54.9 us -> 34.4 us
  starting transfers between devices: 9.12 us -> 25 us
  waiting for transfers between devices: 18.7 us -> 17 us
    all_to_all x2 -> x1, blocking collectives: 43.9 us -> 20.1 us  [local(): gathered = lax.all_to_all(mixed, 'g', 0, 0, tiled=True)]
    ppermute x1, waiting for transfers between devices: 18.7 us -> 0.01 us  [local(): other = lax.ppermute(own, 'h', [(0, 1), (1, 0)])]
    all_to_all x1 -> x2, waiting for transfers between devices: 0.01 us -> 17 us  [the longest x1 13.6 us: local(): arrived = lax.all_to_all(spectra, ('row', 'h', 'k'), 0, 0, tiled=True)]
    all_to_all x1 -> x2, starting transfers between devices: 6.18 us -> 21.8 us  [the longest x1 13.7 us: local(): arrived = lax.all_to_all(projected, 'row', 0, 0, tiled=True)]
    all_to_all x1, blocking collectives: 8.6 us -> 11.5 us  [local(): output = lax.all_to_all(output, ('h', 'k'), 0, 0, tiled=True)]
  transfers between devices with their start and end apart: 2 -> 3, of which waited for: 1 -> 2; matrix products, arithmetic and copies ran while one was open for 0% -> 0% of each run, Pallas kernels for 0% -> 2%
where the time goes in v5:
time: 84.5 us; the launch traced here: 84.2 us
  blocking collectives  34.4 us (41%)
  starting transfers between devices  25 us (30%)
  waiting for transfers between devices  17 us (20%)
  Pallas kernels  7.01 us (8%)
    all_to_all x1, blocking collectives, local(): gathered = lax.all_to_all(mixed, 'g', 0, 0, tiled=True)  20.1 us
    all_to_all x1, starting transfers between devices, local(): arrived = lax.all_to_all(projected, 'row', 0, 0, tiled=True)  13.7 us
    all_to_all x1, waiting for transfers between devices, local(): arrived = lax.all_to_all(spectra, ('row', 'h', 'k'), 0, 0, tiled=True)  13.6 us
    all_to_all x1, blocking collectives, local(): output = lax.all_to_all(output, ('h', 'k'), 0, 0, tiled=True)  11.5 us
    all_to_all x1, starting transfers between devices, local(): arrived = lax.all_to_all(spectra, ('row', 'h', 'k'), 0, 0, tiled=True)  8.03 us
    pallas_call x1, Pallas kernels, project(): pl.pallas_call(project_body, in_specs=[pl.BlockSpec(memory_space=pltpu.HB...  4.08 us
    all_to_all x1, waiting for transfers between devices, local(): arrived = lax.all_to_all(projected, 'row', 0, 0, tiled=True)  3.38 us
    ppermute x1, starting transfers between devices, local(): other = lax.ppermute(own, 'h', [(0, 1), (1, 0)])  3.2 us
  transfers between devices with their start and end apart: 3, of which 2 were waited for; matrix products, arithmetic and copies ran while one was open for 0% of the time, Pallas kernels for 2%

profile of v5, /device:TPU:1, one launch (start us, length us, event | category | flops | bytes accessed | tf_op | source)
XLA Modules:
  0.0 84.2 jit_solution(4747640493919757342)
XLA Ops:
  0.0 0.0 copy-start.3
  0.0 0.0 copy-start.1
  0.0 0.0 copy-start.2
  0.0 0.0 copy-start
  0.0 0.0 copy-start.4
  0.0 4.1 %shard_map.82 = bf16[32,16,128]{2,1,0:T(8,128)(2,1)} custom-call(bf16[1024,2048]{1,0:T(8,128)(2,1)} %x_hbm.1, bf16[64,2048]{1,0:T(8,128)(2,1)} %bitcast.8, f32[1,2048]{1,0:T(1,128)} %bitcast.9), custom_call_target="tpu_custom_call" | custom-call | tf_op jit(solution)/shard_map/pallas_call | solution.py:70
  4.1 13.7 %all-to-all-start = ((bf16[32,16,128]{2,1,0:T(8,128)(2,1)}), bf16[32,16,128]{2,1,0:T(8,128)(2,1)S(1)}, u32[]{:S(2)}, u32[]{:S(2)}) async-start(bf16[32,16,128]{2,1,0:T(8,128)(2,1)} %shard_map.82), calls=%async_computation | async-start | bytes 262144 | tf_op jit(solution)/shard_map/all_to_all | solution.py:210
  17.9 0.0 copy-done.4
  17.9 2.7 %all-gather = bf16[2048,128]{1,0:T(8,128)(2,1)S(1)} all-gather(bf16[1024,128]{1,0:T(8,128)(2,1)S(1)} %copy-done.4), channel_id=2, replica_groups=mesh['row'=32,'g'=4,'h'=2,'k'=2] {'k'}, dimensions={0}, use_global_device_ids=true | all-gather | bytes 786432 | tf_op jit(solution)/shard_map/all_gather | solution.py:207
  20.6 3.2 %collective-permute-start = (bf16[2,1024,128]{2,1,0:T(8,128)(2,1)S(1)}, bf16[2,1024,128]{2,1,0:T(8,128)(2,1)S(1)}, u32[]{:S(2)}, u32[]{:S(2)}) collective-permute-start(bf16[2,1024,128]{2,1,0:T(8,128)(2,1)S(1)} %bitcast.5), channel_id=1, source_target_pairs={{0,2},{2,0},{1,3},{3,1},{4,6},{6,4},{5,7},{7,5},{8,10},{10,8},{9,1... | collective-permute-start | bytes 1572872 | tf_op jit(solution)/shard_map/ppermute | solution.py:208
  23.8 3.4 %all-to-all-done.x_ref = bf16[32,16,128]{2,1,0:T(8,128)(2,1)S(1)} async-done(((bf16[32,16,128]{2,1,0:T(8,128)(2,1)}), bf16[32,16,128]{2,1,0:T(8,128)(2,1)S(1)}, u32[]{:S(2)}, u32[]{:S(2)}) %all-to-all-start) | async-done | bytes 131104 | tf_op jit(solution)/shard_map/all_to_all | solution.py:210
  27.2 0.0 copy-done.3
  27.2 0.0 copy-done.1
  27.2 0.0 copy-done.2
  27.2 1.7 %shard_map.83 = bf16[128,8,128]{2,1,0:T(8,128)(2,1)} custom-call(bf16[32,16,128]{2,1,0:T(8,128)(2,1)S(1)} %all-to-all-done.x_ref, bf16[512,256]{1,0:T(8,128)(2,1)S(1)} %copy-done.2, f32[2,256,128]{2,1,0:T(8,128)S(1)} %copy-done.1, bf16[256,256]{1,0:T(8,128)(2,1)S(1)} %copy-done.3), custom_call_target="tpu_custom_call" | custom-call | tf_op jit(solution)/shard_map/pallas_call | solution.py:133
  28.9 8.0 %all-to-all-start.1 = ((bf16[128,8,128]{2,1,0:T(8,128)(2,1)}), bf16[128,8,128]{2,1,0:T(8,128)(2,1)S(1)}, u32[]{:S(2)}, u32[]{:S(2)}) async-start(bf16[128,8,128]{2,1,0:T(8,128)(2,1)} %shard_map.83), calls=%async_computation.1 | async-start | bytes 524288 | tf_op jit(solution)/shard_map/all_to_all | solution.py:212
  36.9 0.0 collective-permute-done.other_ref
  36.9 13.6 %all-to-all-done.1.x_ref = bf16[128,8,128]{2,1,0:T(8,128)(2,1)S(1)} async-done(((bf16[128,8,128]{2,1,0:T(8,128)(2,1)}), bf16[128,8,128]{2,1,0:T(8,128)(2,1)S(1)}, u32[]{:S(2)}, u32[]{:S(2)}) %all-to-all-start.1) | async-done | bytes 262176 | tf_op jit(solution)/shard_map/all_to_all | solution.py:212
  50.6 0.0 copy-done
  50.6 0.6 shard_map.84
  51.1 20.1 %all_to_all.20.spec_ref = bf16[4,256,256]{2,1,0:T(8,128)(2,1)S(1)} all-to-all(bf16[4,256,256]{2,1,0:T(8,128)(2,1)S(1)} %shard_map.84), channel_id=1, replica_groups=mesh['row'=32,'g'=4,'h'=2,'k'=2] {'g'}, dimensions={0} | all-to-all | bytes 1048576 | tf_op jit(solution)/shard_map/all_to_all | solution.py:216
  71.2 0.7 shard_map.85
  72.0 11.5 %all_to_all.21 = bf16[4,256,128]{2,1,0:T(8,128)(2,1)S(1)} all-to-all(bf16[4,256,128]{2,1,0:T(8,128)(2,1)S(1)} %shard_map.85), channel_id=1, replica_groups=mesh['row'=32,'g'=4,'h'=2,'k'=2] {'h','k'}, dimensions={0} | all-to-all | bytes 524288 | tf_op jit(solution)/shard_map/all_to_all | solution.py:218
  83.5 0.7 copy.10
Async XLA Ops:
  0.0 27.2 %copy-start.3 = (bf16[256,256]{1,0:T(8,128)(2,1)S(1)}, bf16[256,256]{1,0:T(8,128)(2,1)}, u32[]{:S(2)}) copy-start(bf16[256,256]{1,0:T(8,128)(2,1)} %constant.14.clone.two_ref) | copy-start | bytes 393220
  0.0 27.2 %copy-start.1 = (f32[2,256,128]{2,1,0:T(8,128)S(1)}, f32[2,256,128]{2,1,0:T(8,128)}, u32[]{:S(2)}) copy-start(f32[2,256,128]{2,1,0:T(8,128)} %constant.13.clone.turn_ref) | copy-start | bytes 786436
  0.0 27.2 %copy-start.2 = (bf16[512,256]{1,0:T(8,128)(2,1)S(1)}, bf16[512,256]{1,0:T(8,128)(2,1)}, u32[]{:S(2)}) copy-start(bf16[512,256]{1,0:T(8,128)(2,1)} %constant.12.clone.one_ref) | copy-start | bytes 786436
  0.0 50.6 %copy-start = (bf16[256,512]{1,0:T(8,128)(2,1)S(1)}, bf16[256,512]{1,0:T(8,128)(2,1)}, u32[]{:S(2)}) copy-start(bf16[256,512]{1,0:T(8,128)(2,1)} %constant.15.clone.table_ref) | copy-start | bytes 786436
  0.0 17.8 %copy-start.4 = (bf16[1024,128]{1,0:T(8,128)(2,1)S(1)}, bf16[1024,128]{1,0:T(8,128)(2,1)}, u32[]{:S(2)}) copy-start(bf16[1024,128]{1,0:T(8,128)(2,1)} %param.11) | copy-start | bytes 786436
  4.1 23.1 %all-to-all-start = ((bf16[32,16,128]{2,1,0:T(8,128)(2,1)}), bf16[32,16,128]{2,1,0:T(8,128)(2,1)S(1)}, u32[]{:S(2)}, u32[]{:S(2)}) async-start(bf16[32,16,128]{2,1,0:T(8,128)(2,1)} %shard_map.82), calls=%async_computation | async-start | bytes 262144 | tf_op jit(solution)/shard_map/all_to_all | solution.py:210
  20.6 16.3 %collective-permute-start = (bf16[2,1024,128]{2,1,0:T(8,128)(2,1)S(1)}, bf16[2,1024,128]{2,1,0:T(8,128)(2,1)S(1)}, u32[]{:S(2)}, u32[]{:S(2)}) collective-permute-start(bf16[2,1024,128]{2,1,0:T(8,128)(2,1)S(1)} %bitcast.5), channel_id=1, source_target_pairs={{0,2},{2,0},{1,3},{3,1},{4,6},{6,4},{5,7},{7,5},{8,10},{10,8},{9,1... | collective-permute-start | bytes 1572872 | tf_op jit(solution)/shard_map/ppermute | solution.py:208
  28.9 21.7 %all-to-all-start.1 = ((bf16[128,8,128]{2,1,0:T(8,128)(2,1)}), bf16[128,8,128]{2,1,0:T(8,128)(2,1)S(1)}, u32[]{:S(2)}, u32[]{:S(2)}) async-start(bf16[128,8,128]{2,1,0:T(8,128)(2,1)} %shard_map.83), calls=%async_computation.1 | async-start | bytes 524288 | tf_op jit(solution)/shard_map/all_to_all | solution.py:212

commit v6 on v4

--- a/solution.py
+++ b/solution.py
@@ -138,36 +138,45 @@
     )(arrived, *tables)
 
 
-def channel_table(rows, near):
-    source = np.arange(rows * near)
-    channel = np.stack(
-        [(GROUP // near) * (source % near) + source // near + rows * c for c in range(2)]
-    )
+def channel_table(rows):
+    source = np.arange(4 * rows)
+    core, row, half = source // (2 * rows), source // 2 % rows, source % 2
+    place = 2 * half + core
+    channel = np.stack([GROUP // 4 * place + row + rows * c for c in range(2)])
     freq = np.arange(GROUP)
     phase = 2.0 * np.pi * (freq[:, None, None] * channel[None] % GROUP) / GROUP
     both = np.stack([np.cos(phase), np.sin(phase)], 2)
     return jnp.asarray(both.reshape(GROUP, -1), jnp.bfloat16)
 
 
-def channels_body(x_ref, table_ref, out_ref, scr):
-    scr[...] = x_ref[...].astype(jnp.float32)
+def channels_body(core_ref, x_ref, table_ref, out_ref, scr):
+    core = core_ref[0]
+    for k in range(2):
+        part = x_ref[k, :, pl.ds(core, 1)]
+        count = part.shape[0]
+        scr[count * k : count * k + count] = part.reshape(count, *scr.shape[1:]).astype(jnp.float32)
     rows = [
         jnp.concatenate([scr[:, 2 * j, :], scr[:, 2 * j + 1, :]], 1).astype(jnp.bfloat16)
         for j in range(4)
     ]
     data = jnp.concatenate(rows, 0)
     spectrum = jnp.dot(table_ref[...], data, preferred_element_type=jnp.float32)
-    out_ref[...] = jnp.broadcast_to(spectrum.T.astype(jnp.bfloat16)[None], out_ref.shape)
-
-
-def channel_mix(arrived, table, copies):
-    count = arrived.shape[1] * arrived.shape[2] // 4
+    out_ref[...] = spectrum.T.astype(jnp.bfloat16)
+
+
+def channel_mix(core, arrived, table):
+    sources, height, width = arrived.shape[1], *arrived.shape[3:]
     return pl.pallas_call(
         channels_body,
-        out_shape=pltpu.VMEM((copies, count, GROUP), jnp.bfloat16),
-        scratch_shapes=[pltpu.VMEM(arrived.shape, jnp.float32)],
+        in_specs=[
+            pl.BlockSpec(memory_space=pltpu.SMEM),
+            pl.BlockSpec(memory_space=pltpu.VMEM),
+            pl.BlockSpec(memory_space=pltpu.VMEM),
+        ],
+        out_shape=pltpu.VMEM((height * width // 4, GROUP), jnp.bfloat16),
+        scratch_shapes=[pltpu.VMEM((2 * sources, height, width), jnp.float32)],
         compiler_params=SMALL,
-    )(arrived, table)
+    )(core, arrived, table)
 
 
 def output_body(half_ref, spec_ref, own_ref, other_ref, out_ref):
@@ -209,9 +218,11 @@
     projected = project(tokens, w_in, norm_gain)
     arrived = lax.all_to_all(projected, "row", 0, 0, tiled=True)
     spectra = positions(arrived, total)
-    arrived = lax.all_to_all(spectra, ("row", "h", "k"), 0, 0, tiled=True)
-    mixed = channel_mix(arrived, channel_table(rows, 4), 4)
-    gathered = lax.all_to_all(mixed, "g", 0, 0, tiled=True)
+    arrived = lax.all_to_all(spectra, ("row", "h"), 0, 0, tiled=True)
+    arrived = lax.all_gather(arrived.reshape(2 * rows, 2, *arrived.shape[1:]), "k", axis=0)
+    core = lax.axis_index("k").astype(jnp.int32).reshape(1)
+    mixed = channel_mix(core, arrived, channel_table(rows))
+    gathered = lax.all_gather(mixed, "g", axis=0)
     half = lax.axis_index("h").astype(jnp.int32).reshape(1)
     output = output_map(half, gathered, own, other)
     output = lax.all_to_all(output, ("h", "k"), 0, 0, tiled=True)

time: 90.3 us -> 78.1 us (0.86)
  waiting for transfers between devices: 18.7 us -> 3.04 us
  blocking collectives: 54.9 us -> 59.3 us
    all_gather x0 -> x2, blocking collectives: none -> 22 us  [the longest x1 16.2 us: local(): gathered = lax.all_gather(mixed, 'g', axis=0)]
    all_to_all x1 -> x0, blocking collectives: 21 us -> none  [local(): arrived = lax.all_to_all(spectra, ('row', 'h', 'k'), 0, 0, tiled=True)]
    ppermute x1, waiting for transfers between devices: 18.7 us -> 0.01 us  [local(): other = lax.ppermute(own, 'h', [(0, 1), (1, 0)])]
    all_to_all x1, waiting for transfers between devices: 0.01 us -> 3.04 us  [local(): arrived = lax.all_to_all(spectra, ('row', 'h'), 0, 0, tiled=True)]
    all_to_all x1, blocking collectives: 8.6 us -> 10.5 us  [local(): output = lax.all_to_all(output, ('h', 'k'), 0, 0, tiled=True)]
    all_gather x1, blocking collectives: 2.47 us -> 3.9 us  [local(): own = lax.all_gather(w_out, 'k', axis=0)]
    all_to_all x1, starting transfers between devices: 6.18 us -> 5.12 us  [local(): arrived = lax.all_to_all(spectra, ('row', 'h'), 0, 0, tiled=True)]
  transfers between devices with their start and end apart: 2 -> 2, of which waited for: 1 -> 1; matrix products, arithmetic and copies ran while one was open for 0% -> 0% of each run, Pallas kernels for 0% -> 1%
where the time goes in v6:
time: 78.1 us; the launch traced here: 77.8 us
  blocking collectives  59.3 us (76%)
  starting transfers between devices  8.3 us (11%)
  Pallas kernels  6.36 us (8%)
  waiting for transfers between devices  3.04 us (4%)
    all_to_all x1, blocking collectives, local(): arrived = lax.all_to_all(projected, 'row', 0, 0, tiled=True)  22.9 us
    all_gather x1, blocking collectives, local(): gathered = lax.all_gather(mixed, 'g', axis=0)  16.2 us
    all_to_all x1, blocking collectives, local(): output = lax.all_to_all(output, ('h', 'k'), 0, 0, tiled=True)  10.5 us
    all_gather x1, blocking collectives, local(): lax.all_gather(arrived.reshape(2 * rows, 2, *arrived.shape[1:]), 'k', axi...  5.75 us
    all_to_all x1, starting transfers between devices, local(): arrived = lax.all_to_all(spectra, ('row', 'h'), 0, 0, tiled=True)  5.12 us
    all_gather x1, blocking collectives, local(): own = lax.all_gather(w_out, 'k', axis=0)  3.9 us
    pallas_call x1, Pallas kernels, project(): pl.pallas_call(project_body, in_specs=[pl.BlockSpec(memory_space=pltpu.HB...  3.42 us
    ppermute x1, starting transfers between devices, local(): other = lax.ppermute(own, 'h', [(0, 1), (1, 0)])  3.19 us
  transfers between devices with their start and end apart: 2, of which 1 were waited for; matrix products, arithmetic and copies ran while one was open for 0% of the time, Pallas kernels for 1%

profile of v6, /device:TPU:1, one launch (start us, length us, event | category | flops | bytes accessed | tf_op | source)
XLA Modules:
  0.0 77.8 jit_solution(10686611651591725696)
XLA Ops:
  0.0 0.0 copy-start.3
  0.0 0.0 copy-start.1
  0.0 0.0 copy-start.2
  0.0 0.0 copy-start
  0.0 0.0 copy-start.4
  0.0 3.4 %shard_map.82 = bf16[32,16,128]{2,1,0:T(8,128)(2,1)S(1)} custom-call(bf16[1024,2048]{1,0:T(8,128)(2,1)} %x_hbm.1, bf16[64,2048]{1,0:T(8,128)(2,1)} %bitcast.13, f32[1,2048]{1,0:T(1,128)} %bitcast.14), custom_call_target="tpu_custom_call" | custom-call | tf_op jit(solution)/shard_map/pallas_call | solution.py:70
  3.5 22.9 %all_to_all.15.x_ref = bf16[32,16,128]{2,1,0:T(8,128)(2,1)S(1)} all-to-all(bf16[32,16,128]{2,1,0:T(8,128)(2,1)S(1)} %shard_map.82), channel_id=1, replica_groups=mesh['row'=32,'g'=4,'h'=2,'k'=2] {'row'}, dimensions={0} | all-to-all | bytes 262144 | tf_op jit(solution)/shard_map/all_to_all | solution.py:219
  26.3 0.0 copy-done.3
  26.3 0.0 copy-done.1
  26.3 0.0 copy-done.2
  26.3 1.7 %shard_map.83 = bf16[128,8,128]{2,1,0:T(8,128)(2,1)} custom-call(bf16[32,16,128]{2,1,0:T(8,128)(2,1)S(1)} %all_to_all.15.x_ref, bf16[512,256]{1,0:T(8,128)(2,1)S(1)} %copy-done.2, f32[2,256,128]{2,1,0:T(8,128)S(1)} %copy-done.1, bf16[256,256]{1,0:T(8,128)(2,1)S(1)} %copy-done.3), custom_call_target="tpu_custom_call" | custom-call | tf_op jit(solution)/shard_map/pallas_call | solution.py:133
  28.0 5.1 %all-to-all-start.1 = ((bf16[128,8,128]{2,1,0:T(8,128)(2,1)}), bf16[128,8,128]{2,1,0:T(8,128)(2,1)S(1)}, u32[]{:S(2)}, u32[]{:S(2)}) async-start(bf16[128,8,128]{2,1,0:T(8,128)(2,1)} %shard_map.83), calls=%async_computation.1 | async-start | bytes 524288 | tf_op jit(solution)/shard_map/all_to_all | solution.py:221
  33.1 0.0 copy-done.4
  33.1 3.9 %all-gather.1 = bf16[2048,128]{1,0:T(8,128)(2,1)S(1)} all-gather(bf16[1024,128]{1,0:T(8,128)(2,1)S(1)} %copy-done.4), channel_id=3, replica_groups=mesh['row'=32,'g'=4,'h'=2,'k'=2] {'k'}, dimensions={0}, use_global_device_ids=true | all-gather | bytes 786432 | tf_op jit(solution)/shard_map/all_gather | solution.py:216
  37.0 3.2 %collective-permute-start = (bf16[2,1024,128]{2,1,0:T(8,128)(2,1)S(1)}, bf16[2,1024,128]{2,1,0:T(8,128)(2,1)S(1)}, u32[]{:S(2)}, u32[]{:S(2)}) collective-permute-start(bf16[2,1024,128]{2,1,0:T(8,128)(2,1)S(1)} %bitcast.9), channel_id=1, source_target_pairs={{0,2},{2,0},{1,3},{3,1},{4,6},{6,4},{5,7},{7,5},{8,10},{10,8},{9,1... | collective-permute-start | bytes 1572872 | tf_op jit(solution)/shard_map/ppermute | solution.py:217
  40.2 3.0 %all-to-all-done.1 = bf16[128,8,128]{2,1,0:T(8,128)(2,1)S(1)} async-done(((bf16[128,8,128]{2,1,0:T(8,128)(2,1)}), bf16[128,8,128]{2,1,0:T(8,128)(2,1)S(1)}, u32[]{:S(2)}, u32[]{:S(2)}) %all-to-all-start.1) | async-done | bytes 262176 | tf_op jit(solution)/shard_map/all_to_all | solution.py:221
  43.3 5.7 %all_gather.15.x_ref = bf16[2,64,2,8,128]{4,3,2,1,0:T(8,128)(2,1)S(1)} all-gather(bf16[1,64,2,8,128]{4,3,2,1,0:T(8,128)(2,1)S(1)} %bitcast.11), channel_id=1, replica_groups=mesh['row'=32,'g'=4,'h'=2,'k'=2] {'k'}, dimensions={0}, use_global_device_ids=true | all-gather | bytes 786432 | tf_op jit(solution)/shard_map/all_gather | solution.py:222
  49.0 0.0 copy-done
  49.0 0.6 shard_map.84
  49.6 16.2 %all-gather = bf16[1024,256]{1,0:T(8,128)(2,1)S(1)} all-gather(bf16[256,256]{1,0:T(8,128)(2,1)S(1)} %shard_map.84), channel_id=2, replica_groups=mesh['row'=32,'g'=4,'h'=2,'k'=2] {'g'}, dimensions={0}, use_global_device_ids=true | all-gather | bytes 655360 | tf_op jit(solution)/shard_map/all_gather | solution.py:225
  65.8 0.0 collective-permute-done.other_ref
  65.8 0.7 shard_map.85
  66.6 10.5 %all_to_all.16 = bf16[4,256,128]{2,1,0:T(8,128)(2,1)S(1)} all-to-all(bf16[4,256,128]{2,1,0:T(8,128)(2,1)S(1)} %shard_map.85), channel_id=1, replica_groups=mesh['row'=32,'g'=4,'h'=2,'k'=2] {'h','k'}, dimensions={0} | all-to-all | bytes 524288 | tf_op jit(solution)/shard_map/all_to_all | solution.py:228
  77.1 0.7 copy.10
Async XLA Ops:
  0.0 26.3 %copy-start.3 = (bf16[256,256]{1,0:T(8,128)(2,1)S(1)}, bf16[256,256]{1,0:T(8,128)(2,1)}, u32[]{:S(2)}) copy-start(bf16[256,256]{1,0:T(8,128)(2,1)} %constant.16.clone.two_ref) | copy-start | bytes 393220
  0.0 26.3 %copy-start.1 = (f32[2,256,128]{2,1,0:T(8,128)S(1)}, f32[2,256,128]{2,1,0:T(8,128)}, u32[]{:S(2)}) copy-start(f32[2,256,128]{2,1,0:T(8,128)} %constant.15.clone.turn_ref) | copy-start | bytes 786436
  0.0 26.3 %copy-start.2 = (bf16[512,256]{1,0:T(8,128)(2,1)S(1)}, bf16[512,256]{1,0:T(8,128)(2,1)}, u32[]{:S(2)}) copy-start(bf16[512,256]{1,0:T(8,128)(2,1)} %constant.14.clone.one_ref) | copy-start | bytes 786436
  0.0 49.0 %copy-start = (bf16[256,512]{1,0:T(8,128)(2,1)S(1)}, bf16[256,512]{1,0:T(8,128)(2,1)}, u32[]{:S(2)}) copy-start(bf16[256,512]{1,0:T(8,128)(2,1)} %constant.17.clone.table_ref) | copy-start | bytes 786436
  0.0 33.1 %copy-start.4 = (bf16[1024,128]{1,0:T(8,128)(2,1)S(1)}, bf16[1024,128]{1,0:T(8,128)(2,1)}, u32[]{:S(2)}) copy-start(bf16[1024,128]{1,0:T(8,128)(2,1)} %param.11) | copy-start | bytes 786436
  28.0 15.3 %all-to-all-start.1 = ((bf16[128,8,128]{2,1,0:T(8,128)(2,1)}), bf16[128,8,128]{2,1,0:T(8,128)(2,1)S(1)}, u32[]{:S(2)}, u32[]{:S(2)}) async-start(bf16[128,8,128]{2,1,0:T(8,128)(2,1)} %shard_map.83), calls=%async_computation.1 | async-start | bytes 524288 | tf_op jit(solution)/shard_map/all_to_all | solution.py:221
  37.0 28.8 %collective-permute-start = (bf16[2,1024,128]{2,1,0:T(8,128)(2,1)S(1)}, bf16[2,1024,128]{2,1,0:T(8,128)(2,1)S(1)}, u32[]{:S(2)}, u32[]{:S(2)}) collective-permute-start(bf16[2,1024,128]{2,1,0:T(8,128)(2,1)S(1)} %bitcast.9), channel_id=1, source_target_pairs={{0,2},{2,0},{1,3},{3,1},{4,6},{6,4},{5,7},{7,5},{8,10},{10,8},{9,1... | collective-permute-start | bytes 1572872 | tf_op jit(solution)/shard_map/ppermute | solution.py:217

commit v7 on v6

--- a/solution.py
+++ b/solution.py
@@ -8,6 +8,7 @@
 from jax.experimental.pallas import tpu as pltpu
 from jax.sharding import Mesh
 from jax.sharding import PartitionSpec as P
+
 
 GROUP = 256
 NORM_EPS = 1e-06
@@ -213,17 +214,18 @@
 def local(tokens, norm_gain, w_in, w_out):
     rows = lax.axis_size("row")
     total = tokens.shape[0] * rows
+    other = lax.ppermute(w_out, "h", [(0, 1), (1, 0)])
     own = lax.all_gather(w_out, "k", axis=0)
-    other = lax.ppermute(own, "h", [(0, 1), (1, 0)])
+    other = lax.all_gather(other, "k", axis=0)
     projected = project(tokens, w_in, norm_gain)
     arrived = lax.all_to_all(projected, "row", 0, 0, tiled=True)
+    half, core = (lax.axis_index(name).astype(jnp.int32).reshape(1) for name in ("h", "k"))
+    arrived, half, core = lax.optimization_barrier((arrived, half, core))
     spectra = positions(arrived, total)
     arrived = lax.all_to_all(spectra, ("row", "h"), 0, 0, tiled=True)
     arrived = lax.all_gather(arrived.reshape(2 * rows, 2, *arrived.shape[1:]), "k", axis=0)
-    core = lax.axis_index("k").astype(jnp.int32).reshape(1)
     mixed = channel_mix(core, arrived, channel_table(rows))
     gathered = lax.all_gather(mixed, "g", axis=0)
-    half = lax.axis_index("h").astype(jnp.int32).reshape(1)
     output = output_map(half, gathered, own, other)
     output = lax.all_to_all(output, ("h", "k"), 0, 0, tiled=True)
     return output.reshape(tokens.shape[0], w_out.shape[1])

time: 78.1 us -> 79.4 us (1.017)
  blocking collectives: 59.3 us -> 37.4 us
  starting transfers between devices: 8.3 us -> 21.8 us
  waiting for transfers between devices: 3.04 us -> 12.1 us
    all_to_all x1 -> x0, blocking collectives: 22.9 us -> none  [local(): arrived = lax.all_to_all(projected, 'row', 0, 0, tiled=True)]
    all_to_all x0 -> x1, starting transfers between devices: none -> 13.7 us  [local(): arrived = lax.all_to_all(projected, 'row', 0, 0, tiled=True)]
    all_to_all x0 -> x1, waiting for transfers between devices: none -> 9.34 us  [local(): arrived = lax.all_to_all(projected, 'row', 0, 0, tiled=True)]
    all_gather x0 -> x1, blocking collectives: none -> 3.64 us  [local(): other = lax.all_gather(other, 'k', axis=0)]
    all_gather x1, blocking collectives: 5.75 us -> 2.23 us  [local(): lax.all_gather(arrived.reshape(2 * rows, 2, *arrived.shape[1:]), 'k', axi...]
    all_to_all x1, waiting for transfers between devices: 3.04 us -> 0.01 us  [local(): arrived = lax.all_to_all(spectra, ('row', 'h'), 0, 0, tiled=True)]
    ppermute x1, waiting for transfers between devices: 0.01 us -> 2.78 us  [local(): other = lax.ppermute(w_out, 'h', [(0, 1), (1, 0)])]
  transfers between devices with their start and end apart: 2 -> 3, of which waited for: 1 -> 2; matrix products, arithmetic and copies ran while one was open for 0% -> 0% of each run, Pallas kernels for 1% -> 0%
where the time goes in v7:
time: 79.4 us; the launch traced here: 79.1 us
  blocking collectives  37.4 us (47%)
  starting transfers between devices  21.8 us (27%)
  waiting for transfers between devices  12.1 us (15%)
  Pallas kernels  7.01 us (9%)
    all_gather x1, blocking collectives, local(): gathered = lax.all_gather(mixed, 'g', axis=0)  16.3 us
    all_to_all x1, starting transfers between devices, local(): arrived = lax.all_to_all(projected, 'row', 0, 0, tiled=True)  13.7 us
    all_to_all x1, blocking collectives, local(): output = lax.all_to_all(output, ('h', 'k'), 0, 0, tiled=True)  10.8 us
    all_to_all x1, waiting for transfers between devices, local(): arrived = lax.all_to_all(projected, 'row', 0, 0, tiled=True)  9.34 us
    all_to_all x1, starting transfers between devices, local(): arrived = lax.all_to_all(spectra, ('row', 'h'), 0, 0, tiled=True)  5.12 us
    all_gather x1, blocking collectives, local(): own = lax.all_gather(w_out, 'k', axis=0)  4.47 us
    pallas_call x1, Pallas kernels, project(): pl.pallas_call(project_body, in_specs=[pl.BlockSpec(memory_space=pltpu.HB...  4.08 us
    all_gather x1, blocking collectives, local(): other = lax.all_gather(other, 'k', axis=0)  3.64 us
  transfers between devices with their start and end apart: 3, of which 2 were waited for; matrix products, arithmetic and copies ran while one was open for 0% of the time, Pallas kernels for 0%

profile of v7, /device:TPU:1, one launch (start us, length us, event | category | flops | bytes accessed | tf_op | source)
XLA Modules:
  0.0 79.1 jit_solution(3953992255219451204)
XLA Ops:
  0.0 0.0 copy-start.3
  0.0 0.0 copy-start.1
  0.0 0.0 copy-start.2
  0.0 0.0 copy-start.4
  0.0 0.0 copy-start
  0.0 4.1 %shard_map.82 = bf16[32,16,128]{2,1,0:T(8,128)(2,1)} custom-call(bf16[1024,2048]{1,0:T(8,128)(2,1)} %x_hbm.1, bf16[64,2048]{1,0:T(8,128)(2,1)} %bitcast.14, f32[1,2048]{1,0:T(1,128)} %bitcast.15), custom_call_target="tpu_custom_call" | custom-call | tf_op jit(solution)/shard_map/pallas_call | solution.py:71
  4.1 13.7 %all-to-all-start = ((bf16[32,16,128]{2,1,0:T(8,128)(2,1)}), bf16[32,16,128]{2,1,0:T(8,128)(2,1)S(1)}, u32[]{:S(2)}, u32[]{:S(2)}) async-start(bf16[32,16,128]{2,1,0:T(8,128)(2,1)} %shard_map.82), calls=%async_computation | async-start | bytes 262144 | tf_op jit(solution)/shard_map/all_to_all | solution.py:221
  17.9 9.3 %all-to-all-done.x_ref = bf16[32,16,128]{2,1,0:T(8,128)(2,1)S(1)} async-done(((bf16[32,16,128]{2,1,0:T(8,128)(2,1)}), bf16[32,16,128]{2,1,0:T(8,128)(2,1)S(1)}, u32[]{:S(2)}, u32[]{:S(2)}) %all-to-all-start) | async-done | bytes 131104 | tf_op jit(solution)/shard_map/all_to_all | solution.py:221
  27.2 0.0 copy-done.3
  27.2 0.0 copy-done.1
  27.2 0.0 copy-done.2
  27.2 1.7 %shard_map.83 = bf16[128,8,128]{2,1,0:T(8,128)(2,1)} custom-call(bf16[32,16,128]{2,1,0:T(8,128)(2,1)S(1)} %all-to-all-done.x_ref, bf16[512,256]{1,0:T(8,128)(2,1)S(1)} %copy-done.2, f32[2,256,128]{2,1,0:T(8,128)S(1)} %copy-done.1, bf16[256,256]{1,0:T(8,128)(2,1)S(1)} %copy-done.3), custom_call_target="tpu_custom_call" | custom-call | tf_op jit(solution)/shard_map/pallas_call | solution.py:134
  28.9 5.1 %all-to-all-start.1 = ((bf16[128,8,128]{2,1,0:T(8,128)(2,1)}), bf16[128,8,128]{2,1,0:T(8,128)(2,1)S(1)}, u32[]{:S(2)}, u32[]{:S(2)}) async-start(bf16[128,8,128]{2,1,0:T(8,128)(2,1)} %shard_map.83), calls=%async_computation.1 | async-start | bytes 524288 | tf_op jit(solution)/shard_map/all_to_all | solution.py:225
  34.0 0.0 copy-done.4
  34.0 2.9 %collective-permute-start = (bf16[1024,128]{1,0:T(8,128)(2,1)S(1)}, bf16[1024,128]{1,0:T(8,128)(2,1)S(1)}, u32[]{:S(2)}, u32[]{:S(2)}) collective-permute-start(bf16[1024,128]{1,0:T(8,128)(2,1)S(1)} %copy-done.4), channel_id=1, source_target_pairs={{0,2},{2,0},{1,3},{3,1},{4,6},{6,4},{5,7},{7,5},{8,10},{10,8},{9,1... | collective-permute-start | bytes 786440 | tf_op jit(solution)/shard_map/ppermute | solution.py:217
  36.9 4.5 %all-gather.1 = bf16[2048,128]{1,0:T(8,128)(2,1)S(1)} all-gather(bf16[1024,128]{1,0:T(8,128)(2,1)S(1)} %copy-done.4), channel_id=3, replica_groups=mesh['row'=32,'g'=4,'h'=2,'k'=2] {'k'}, dimensions={0}, use_global_device_ids=true | all-gather | bytes 786432 | tf_op jit(solution)/shard_map/all_gather | solution.py:218
  41.4 2.8 %collective-permute-done = bf16[1024,128]{1,0:T(8,128)(2,1)S(1)} collective-permute-done((bf16[1024,128]{1,0:T(8,128)(2,1)S(1)}, bf16[1024,128]{1,0:T(8,128)(2,1)S(1)}, u32[]{:S(2)}, u32[]{:S(2)}) %collective-permute-start) | collective-permute-done | bytes 262176 | tf_op jit(solution)/shard_map/ppermute | solution.py:217
  44.2 3.6 %all-gather.2 = bf16[2048,128]{1,0:T(8,128)(2,1)S(1)} all-gather(bf16[1024,128]{1,0:T(8,128)(2,1)S(1)} %collective-permute-done), channel_id=4, replica_groups=mesh['row'=32,'g'=4,'h'=2,'k'=2] {'k'}, dimensions={0}, use_global_device_ids=true | all-gather | bytes 786432 | tf_op jit(solution)/shard_map/all_gather | solution.py:219
  47.8 0.0 all-to-all-done.1
  47.8 2.2 %all_gather.21.x_ref = bf16[2,64,2,8,128]{4,3,2,1,0:T(8,128)(2,1)S(1)} all-gather(bf16[1,64,2,8,128]{4,3,2,1,0:T(8,128)(2,1)S(1)} %bitcast.12), channel_id=1, replica_groups=mesh['row'=32,'g'=4,'h'=2,'k'=2] {'k'}, dimensions={0}, use_global_device_ids=true | all-gather | bytes 786432 | tf_op jit(solution)/shard_map/all_gather | solution.py:226
  50.1 0.0 copy-done
  50.1 0.6 shard_map.84
  50.6 16.3 %all-gather = bf16[1024,256]{1,0:T(8,128)(2,1)S(1)} all-gather(bf16[256,256]{1,0:T(8,128)(2,1)S(1)} %shard_map.84), channel_id=2, replica_groups=mesh['row'=32,'g'=4,'h'=2,'k'=2] {'g'}, dimensions={0}, use_global_device_ids=true | all-gather | bytes 655360 | tf_op jit(solution)/shard_map/all_gather | solution.py:228
  66.9 0.7 shard_map.85
  67.6 10.8 %all_to_all.15 = bf16[4,256,128]{2,1,0:T(8,128)(2,1)S(1)} all-to-all(bf16[4,256,128]{2,1,0:T(8,128)(2,1)S(1)} %shard_map.85), channel_id=1, replica_groups=mesh['row'=32,'g'=4,'h'=2,'k'=2] {'h','k'}, dimensions={0} | all-to-all | bytes 524288 | tf_op jit(solution)/shard_map/all_to_all | solution.py:230
  78.4 0.7 copy.10
Async XLA Ops:
  0.0 27.2 %copy-start.3 = (bf16[256,256]{1,0:T(8,128)(2,1)S(1)}, bf16[256,256]{1,0:T(8,128)(2,1)}, u32[]{:S(2)}) copy-start(bf16[256,256]{1,0:T(8,128)(2,1)} %constant.16.clone.two_ref) | copy-start | bytes 393220
  0.0 27.2 %copy-start.1 = (f32[2,256,128]{2,1,0:T(8,128)S(1)}, f32[2,256,128]{2,1,0:T(8,128)}, u32[]{:S(2)}) copy-start(f32[2,256,128]{2,1,0:T(8,128)} %constant.15.clone.turn_ref) | copy-start | bytes 786436
  0.0 27.2 %copy-start.2 = (bf16[512,256]{1,0:T(8,128)(2,1)S(1)}, bf16[512,256]{1,0:T(8,128)(2,1)}, u32[]{:S(2)}) copy-start(bf16[512,256]{1,0:T(8,128)(2,1)} %constant.14.clone.one_ref) | copy-start | bytes 786436
  0.0 34.0 %copy-start.4 = (bf16[1024,128]{1,0:T(8,128)(2,1)S(1)}, bf16[1024,128]{1,0:T(8,128)(2,1)}, u32[]{:S(2)}) copy-start(bf16[1024,128]{1,0:T(8,128)(2,1)} %param.11) | copy-start | bytes 786436
  0.0 50.1 %copy-start = (bf16[256,512]{1,0:T(8,128)(2,1)S(1)}, bf16[256,512]{1,0:T(8,128)(2,1)}, u32[]{:S(2)}) copy-start(bf16[256,512]{1,0:T(8,128)(2,1)} %constant.17.clone.table_ref) | copy-start | bytes 786436
  4.1 23.1 %all-to-all-start = ((bf16[32,16,128]{2,1,0:T(8,128)(2,1)}), bf16[32,16,128]{2,1,0:T(8,128)(2,1)S(1)}, u32[]{:S(2)}, u32[]{:S(2)}) async-start(bf16[32,16,128]{2,1,0:T(8,128)(2,1)} %shard_map.82), calls=%async_computation | async-start | bytes 262144 | tf_op jit(solution)/shard_map/all_to_all | solution.py:221
  28.9 19.0 %all-to-all-start.1 = ((bf16[128,8,128]{2,1,0:T(8,128)(2,1)}), bf16[128,8,128]{2,1,0:T(8,128)(2,1)S(1)}, u32[]{:S(2)}, u32[]{:S(2)}) async-start(bf16[128,8,128]{2,1,0:T(8,128)(2,1)} %shard_map.83), calls=%async_computation.1 | async-start | bytes 524288 | tf_op jit(solution)/shard_map/all_to_all | solution.py:225
  34.0 10.2 %collective-permute-start = (bf16[1024,128]{1,0:T(8,128)(2,1)S(1)}, bf16[1024,128]{1,0:T(8,128)(2,1)S(1)}, u32[]{:S(2)}, u32[]{:S(2)}) collective-permute-start(bf16[1024,128]{1,0:T(8,128)(2,1)S(1)} %copy-done.4), channel_id=1, source_target_pairs={{0,2},{2,0},{1,3},{3,1},{4,6},{6,4},{5,7},{7,5},{8,10},{10,8},{9,1... | collective-permute-start | bytes 786440 | tf_op jit(solution)/shard_map/ppermute | solution.py:217

commit v8 on v6

--- a/solution.py
+++ b/solution.py
@@ -8,6 +8,7 @@
 from jax.experimental.pallas import tpu as pltpu
 from jax.sharding import Mesh
 from jax.sharding import PartitionSpec as P
+
 
 GROUP = 256
 NORM_EPS = 1e-06
@@ -153,7 +154,7 @@
     core = core_ref[0]
     for k in range(2):
         part = x_ref[k, :, pl.ds(core, 1)]
-        count = part.shape[0]
+        count = 2 * part.shape[0]
         scr[count * k : count * k + count] = part.reshape(count, *scr.shape[1:]).astype(jnp.float32)
     rows = [
         jnp.concatenate([scr[:, 2 * j, :], scr[:, 2 * j + 1, :]], 1).astype(jnp.bfloat16)
@@ -165,7 +166,7 @@
 
 
 def channel_mix(core, arrived, table):
-    sources, height, width = arrived.shape[1], *arrived.shape[3:]
+    sources, height, width = 2 * arrived.shape[1], *arrived.shape[4:]
     return pl.pallas_call(
         channels_body,
         in_specs=[
@@ -179,59 +180,57 @@
     )(core, arrived, table)
 
 
-def output_body(half_ref, spec_ref, own_ref, other_ref, out_ref):
-    half = half_ref[0]
+def output_body(chip_ref, spec_ref, *refs):
+    *weights, out_ref = refs
     groups = spec_ref.shape[0]
-    for k in range(2):
-        for ref, place in ((own_ref, 2 * half + k), (other_ref, 2 * (1 - half) + k)):
-            total = None
-            for g in range(groups):
-                part = jnp.dot(
-                    spec_ref[g],
-                    ref[k, GROUP * g : GROUP * g + GROUP, :],
-                    preferred_element_type=jnp.float32,
-                )
-                total = part if total is None else total + part
-            out_ref[pl.ds(place, 1)] = total.astype(jnp.bfloat16)[None]
-
-
-def output_map(half, gathered, own, other):
+    for flip, ref in enumerate(weights):
+        total = None
+        for g in range(groups):
+            part = jnp.dot(
+                spec_ref[g],
+                ref[GROUP * g : GROUP * g + GROUP, :],
+                preferred_element_type=jnp.float32,
+            )
+            total = part if total is None else total + part
+        out_ref[pl.ds(chip_ref[0] ^ flip, 1)] = total.astype(jnp.bfloat16)[None]
+
+
+def output_map(chip, gathered, *weights):
     count = gathered.shape[1]
+    whole = pl.BlockSpec(memory_space=pltpu.VMEM)
     return pl.pallas_call(
         output_body,
-        in_specs=[
-            pl.BlockSpec(memory_space=pltpu.SMEM),
-            pl.BlockSpec(memory_space=pltpu.VMEM),
-            pl.BlockSpec(memory_space=pltpu.VMEM),
-            pl.BlockSpec(memory_space=pltpu.VMEM),
-        ],
-        out_shape=pltpu.VMEM((4, count, own.shape[2]), jnp.bfloat16),
+        in_specs=[pl.BlockSpec(memory_space=pltpu.SMEM)] + [whole] * (1 + len(weights)),
+        out_shape=pltpu.VMEM((len(weights), count, weights[0].shape[1]), jnp.bfloat16),
         compiler_params=SMALL,
-    )(half, gathered, own, other)
+    )(chip, gathered, *weights)
 
 
 def local(tokens, norm_gain, w_in, w_out):
     rows = lax.axis_size("row")
     total = tokens.shape[0] * rows
-    own = lax.all_gather(w_out, "k", axis=0)
-    other = lax.ppermute(own, "h", [(0, 1), (1, 0)])
+    flips = ((("h",), 1), (("g0",), 1), (("g0", "h"), 3))
+    near = [
+        lax.ppermute(w_out, axes, [(i, i ^ flip) for i in range(2 * len(axes))])
+        for axes, flip in flips
+    ]
     projected = project(tokens, w_in, norm_gain)
     arrived = lax.all_to_all(projected, "row", 0, 0, tiled=True)
     spectra = positions(arrived, total)
-    arrived = lax.all_to_all(spectra, ("row", "h"), 0, 0, tiled=True)
-    arrived = lax.all_gather(arrived.reshape(2 * rows, 2, *arrived.shape[1:]), "k", axis=0)
+    arrived = lax.all_to_all(spectra, ("row", "g0", "h"), 0, 0, tiled=True)
+    arrived = lax.all_gather(arrived.reshape(rows, 2, 2, *arrived.shape[1:]), "k", axis=0)
     core = lax.axis_index("k").astype(jnp.int32).reshape(1)
     mixed = channel_mix(core, arrived, channel_table(rows))
-    gathered = lax.all_gather(mixed, "g", axis=0)
-    half = lax.axis_index("h").astype(jnp.int32).reshape(1)
-    output = output_map(half, gathered, own, other)
-    output = lax.all_to_all(output, ("h", "k"), 0, 0, tiled=True)
+    gathered = lax.all_gather(mixed, ("g1", "k"), axis=0)
+    chip = lax.axis_index(("g0", "h")).astype(jnp.int32).reshape(1)
+    output = output_map(chip, gathered, w_out, *near)
+    output = lax.all_to_all(output, ("g0", "h"), 0, 0, tiled=True)
     return output.reshape(tokens.shape[0], w_out.shape[1])
 
 
 def solution(mesh):
-    mesh = Mesh(mesh.devices.reshape(32, 4, 2, 2), ("row", "g", "h", "k"))
-    columns = ("g", "h", "k")
+    mesh = Mesh(mesh.devices.reshape(32, 2, 2, 2, 2), ("row", "g1", "g0", "h", "k"))
+    columns = ("g1", "g0", "h", "k")
     placed = (P("row", None), P(), P(None, columns), P(None, columns))
     return jax.shard_map(
         local, mesh=mesh, in_specs=placed, out_specs=P("row", columns), check_vma=False

time: 78.1 us -> 87.1 us (1.12)
  starting transfers between devices: 8.3 us -> 17.6 us
    ppermute x1 -> x3, starting transfers between devices: 3.19 us -> 9.27 us  [local(): lax.ppermute(w_out, axes, [(i, i ^ flip) for i in range(2 * len(axes))])]
    all_to_all x1, starting transfers between devices: 5.12 us -> 8.37 us  [local(): arrived = lax.all_to_all(spectra, ('row', 'g0', 'h'), 0, 0, tiled=True)]
    all_gather x3 -> x2, blocking collectives: 25.9 us -> 25.5 us  [the longest x1 14 us: local(): gathered = lax.all_gather(mixed, ('g1', 'k'), axis=0)]
  transfers between devices with their start and end apart: 2 -> 4, of which waited for: 1 -> 1; matrix products, arithmetic and copies ran while one was open for 0% -> 0% of each run, Pallas kernels for 1% -> 1%
where the time goes in v8:
time: 87.1 us; the launch traced here: 86.8 us
  blocking collectives  59 us (68%)
  starting transfers between devices  17.6 us (20%)
  Pallas kernels  6.36 us (7%)
  waiting for transfers between devices  2.91 us (3%)
    all_to_all x1, blocking collectives, local(): arrived = lax.all_to_all(projected, 'row', 0, 0, tiled=True)  22.9 us
    all_gather x1, blocking collectives, local(): gathered = lax.all_gather(mixed, ('g1', 'k'), axis=0)  14 us
    all_gather x1, blocking collectives, local(): lax.all_gather(arrived.reshape(rows, 2, 2, *arrived.shape[1:]), 'k', axis=0)  11.5 us
    all_to_all x1, blocking collectives, local(): output = lax.all_to_all(output, ('g0', 'h'), 0, 0, tiled=True)  10.7 us
    ppermute x3, starting transfers between devices, local(): lax.ppermute(w_out, axes, [(i, i ^ flip) for i in range(2 * len(axes))])  9.27 us
    all_to_all x1, starting transfers between devices, local(): arrived = lax.all_to_all(spectra, ('row', 'g0', 'h'), 0, 0, tiled=True)  8.37 us
    pallas_call x1, Pallas kernels, project(): pl.pallas_call(project_body, in_specs=[pl.BlockSpec(memory_space=pltpu.HB...  3.42 us
    all_to_all x1, waiting for transfers between devices, local(): arrived = lax.all_to_all(spectra, ('row', 'g0', 'h'), 0, 0, tiled=True)  2.91 us
  transfers between devices with their start and end apart: 4, of which 1 were waited for; matrix products, arithmetic and copies ran while one was open for 0% of the time, Pallas kernels for 1%

profile of v8, /device:TPU:1, one launch (start us, length us, event | category | flops | bytes accessed | tf_op | source)
XLA Modules:
  0.0 86.8 jit_solution(7962288730033231178)
XLA Ops:
  0.0 0.0 copy-start.4
  0.0 0.0 copy-start.2
  0.0 0.0 copy-start.3
  0.0 0.0 copy-start
  0.0 0.0 copy-start.1
  0.0 3.4 %shard_map.82 = bf16[32,16,128]{2,1,0:T(8,128)(2,1)S(1)} custom-call(bf16[1024,2048]{1,0:T(8,128)(2,1)} %x_hbm.1, bf16[64,2048]{1,0:T(8,128)(2,1)} %bitcast.10, f32[1,2048]{1,0:T(1,128)} %bitcast.11), custom_call_target="tpu_custom_call" | custom-call | tf_op jit(solution)/shard_map/pallas_call | solution.py:71
  3.5 22.9 %all_to_all.15.x_ref = bf16[32,16,128]{2,1,0:T(8,128)(2,1)S(1)} all-to-all(bf16[32,16,128]{2,1,0:T(8,128)(2,1)S(1)} %shard_map.82), channel_id=1, replica_groups=mesh['row'=32,'g1'=2,'g0'=2,'h'=2,'k'=2] {'row'}, dimensions={0} | all-to-all | bytes 262144 | tf_op jit(solution)/shard_map/all_to_all | solution.py:218
  26.3 0.0 copy-done.4
  26.3 0.0 copy-done.2
  26.3 0.0 copy-done.3
  26.3 1.7 %shard_map.83 = bf16[128,8,128]{2,1,0:T(8,128)(2,1)} custom-call(bf16[32,16,128]{2,1,0:T(8,128)(2,1)S(1)} %all_to_all.15.x_ref, bf16[512,256]{1,0:T(8,128)(2,1)S(1)} %copy-done.3, f32[2,256,128]{2,1,0:T(8,128)S(1)} %copy-done.2, bf16[256,256]{1,0:T(8,128)(2,1)S(1)} %copy-done.4), custom_call_target="tpu_custom_call" | custom-call | tf_op jit(solution)/shard_map/pallas_call | solution.py:134
  28.0 8.4 %all-to-all-start.1 = ((bf16[128,8,128]{2,1,0:T(8,128)(2,1)}), bf16[128,8,128]{2,1,0:T(8,128)(2,1)S(1)}, u32[]{:S(2)}, u32[]{:S(2)}) async-start(bf16[128,8,128]{2,1,0:T(8,128)(2,1)} %shard_map.83), calls=%async_computation.1 | async-start | bytes 524288 | tf_op jit(solution)/shard_map/all_to_all | solution.py:220
  36.4 0.0 copy-done.1
  36.4 3.4 %collective-permute-start.1 = (bf16[1024,128]{1,0:T(8,128)(2,1)S(1)}, bf16[1024,128]{1,0:T(8,128)(2,1)S(1)}, u32[]{:S(2)}, u32[]{:S(2)}) collective-permute-start(bf16[1024,128]{1,0:T(8,128)(2,1)S(1)} %copy-done.1), channel_id=1, source_target_pairs={{0,4},{4,0},{1,5},{5,1},{2,6},{6,2},{3,7},{7,3},{8,12},{12,8},{9,1... | collective-permute-start | bytes 786440 | tf_op jit(solution)/shard_map/ppermute | solution.py:214
  39.8 3.1 %collective-permute-start = (bf16[1024,128]{1,0:T(8,128)(2,1)S(1)}, bf16[1024,128]{1,0:T(8,128)(2,1)S(1)}, u32[]{:S(2)}, u32[]{:S(2)}) collective-permute-start(bf16[1024,128]{1,0:T(8,128)(2,1)S(1)} %copy-done.1), channel_id=1, source_target_pairs={{0,2},{2,0},{1,3},{3,1},{4,6},{6,4},{5,7},{7,5},{8,10},{10,8},{9,1... | collective-permute-start | bytes 786440 | tf_op jit(solution)/shard_map/ppermute | solution.py:214
  42.9 2.8 %collective-permute-start.2 = (bf16[1024,128]{1,0:T(8,128)(2,1)S(1)}, bf16[1024,128]{1,0:T(8,128)(2,1)S(1)}, u32[]{:S(2)}, u32[]{:S(2)}) collective-permute-start(bf16[1024,128]{1,0:T(8,128)(2,1)S(1)} %copy-done.1), channel_id=1, source_target_pairs={{0,6},{2,4},{4,2},{6,0},{1,7},{3,5},{5,3},{7,1},{8,14},{10,12},{12... | collective-permute-start | bytes 786440 | tf_op jit(solution)/shard_map/ppermute | solution.py:214
  45.7 2.9 %all-to-all-done.1 = bf16[128,8,128]{2,1,0:T(8,128)(2,1)S(1)} async-done(((bf16[128,8,128]{2,1,0:T(8,128)(2,1)}), bf16[128,8,128]{2,1,0:T(8,128)(2,1)S(1)}, u32[]{:S(2)}, u32[]{:S(2)}) %all-to-all-start.1) | async-done | bytes 262176 | tf_op jit(solution)/shard_map/all_to_all | solution.py:220
  48.6 11.5 %all_gather.9.x_ref = bf16[2,32,2,2,8,128]{5,4,3,2,1,0:T(8,128)(2,1)S(1)} all-gather(bf16[1,32,2,2,8,128]{5,4,3,2,1,0:T(8,128)(2,1)S(1)} %bitcast.8), channel_id=1, replica_groups=mesh['row'=32,'g1'=2,'g0'=2,'h'=2,'k'=2] {'k'}, dimensions={0}, use_global_device_ids=true | all-gather | bytes 786432 | tf_op jit(solution)/shard_map/all_gather | solution.py:221
  60.1 0.0 copy-done
  60.1 0.6 shard_map.84
  60.7 14.0 %all-gather = bf16[1024,256]{1,0:T(8,128)(2,1)S(1)} all-gather(bf16[256,256]{1,0:T(8,128)(2,1)S(1)} %shard_map.84), channel_id=2, replica_groups=mesh['row'=32,'g1'=2,'g0'=2,'h'=2,'k'=2] {'g1','k'}, dimensions={0}, use_global_device_ids=true | all-gather | bytes 655360 | tf_op jit(solution)/shard_map/all_gather | solution.py:224
  74.7 0.0 collective-permute-done.1.refs_2_
  74.7 0.0 collective-permute-done.refs_1_
  74.7 0.0 collective-permute-done.2.refs_3_
  74.7 0.7 shard_map.85
  75.4 10.7 %all_to_all.16 = bf16[4,256,128]{2,1,0:T(8,128)(2,1)S(1)} all-to-all(bf16[4,256,128]{2,1,0:T(8,128)(2,1)S(1)} %shard_map.85), channel_id=1, replica_groups=mesh['row'=32,'g1'=2,'g0'=2,'h'=2,'k'=2] {'g0','h'}, dimensions={0} | all-to-all | bytes 524288 | tf_op jit(solution)/shard_map/all_to_all | solution.py:227
  86.1 0.7 copy.10
Async XLA Ops:
  0.0 26.3 %copy-start.4 = (bf16[256,256]{1,0:T(8,128)(2,1)S(1)}, bf16[256,256]{1,0:T(8,128)(2,1)}, u32[]{:S(2)}) copy-start(bf16[256,256]{1,0:T(8,128)(2,1)} %constant.22.clone.two_ref) | copy-start | bytes 393220
  0.0 26.3 %copy-start.2 = (f32[2,256,128]{2,1,0:T(8,128)S(1)}, f32[2,256,128]{2,1,0:T(8,128)}, u32[]{:S(2)}) copy-start(f32[2,256,128]{2,1,0:T(8,128)} %constant.21.clone.turn_ref) | copy-start | bytes 786436
  0.0 26.3 %copy-start.3 = (bf16[512,256]{1,0:T(8,128)(2,1)S(1)}, bf16[512,256]{1,0:T(8,128)(2,1)}, u32[]{:S(2)}) copy-start(bf16[512,256]{1,0:T(8,128)(2,1)} %constant.20.clone.one_ref) | copy-start | bytes 786436
  0.0 60.1 %copy-start = (bf16[256,512]{1,0:T(8,128)(2,1)S(1)}, bf16[256,512]{1,0:T(8,128)(2,1)}, u32[]{:S(2)}) copy-start(bf16[256,512]{1,0:T(8,128)(2,1)} %constant.23.clone.table_ref) | copy-start | bytes 786436
  0.0 36.4 %copy-start.1 = (bf16[1024,128]{1,0:T(8,128)(2,1)S(1)}, bf16[1024,128]{1,0:T(8,128)(2,1)}, u32[]{:S(2)}) copy-start(bf16[1024,128]{1,0:T(8,128)(2,1)} %refs_0_.1) | copy-start | bytes 786436
  28.0 20.6 %all-to-all-start.1 = ((bf16[128,8,128]{2,1,0:T(8,128)(2,1)}), bf16[128,8,128]{2,1,0:T(8,128)(2,1)S(1)}, u32[]{:S(2)}, u32[]{:S(2)}) async-start(bf16[128,8,128]{2,1,0:T(8,128)(2,1)} %shard_map.83), calls=%async_computation.1 | async-start | bytes 524288 | tf_op jit(solution)/shard_map/all_to_all | solution.py:220
  36.4 38.3 %collective-permute-start.1 = (bf16[1024,128]{1,0:T(8,128)(2,1)S(1)}, bf16[1024,128]{1,0:T(8,128)(2,1)S(1)}, u32[]{:S(2)}, u32[]{:S(2)}) collective-permute-start(bf16[1024,128]{1,0:T(8,128)(2,1)S(1)} %copy-done.1), channel_id=1, source_target_pairs={{0,4},{4,0},{1,5},{5,1},{2,6},{6,2},{3,7},{7,3},{8,12},{12,8},{9,1... | collective-permute-start | bytes 786440 | tf_op jit(solution)/shard_map/ppermute | solution.py:214
  39.8 34.9 %collective-permute-start = (bf16[1024,128]{1,0:T(8,128)(2,1)S(1)}, bf16[1024,128]{1,0:T(8,128)(2,1)S(1)}, u32[]{:S(2)}, u32[]{:S(2)}) collective-permute-start(bf16[1024,128]{1,0:T(8,128)(2,1)S(1)} %copy-done.1), channel_id=1, source_target_pairs={{0,2},{2,0},{1,3},{3,1},{4,6},{6,4},{5,7},{7,5},{8,10},{10,8},{9,1... | collective-permute-start | bytes 786440 | tf_op jit(solution)/shard_map/ppermute | solution.py:214
  42.9 31.8 %collective-permute-start.2 = (bf16[1024,128]{1,0:T(8,128)(2,1)S(1)}, bf16[1024,128]{1,0:T(8,128)(2,1)S(1)}, u32[]{:S(2)}, u32[]{:S(2)}) collective-permute-start(bf16[1024,128]{1,0:T(8,128)(2,1)S(1)} %copy-done.1), channel_id=1, source_target_pairs={{0,6},{2,4},{4,2},{6,0},{1,7},{3,5},{5,3},{7,1},{8,14},{10,12},{12... | collective-permute-start | bytes 786440 | tf_op jit(solution)/shard_map/ppermute | solution.py:214

commit v9 on v6

--- a/solution.py
+++ b/solution.py
@@ -181,18 +181,14 @@
 
 def output_body(half_ref, spec_ref, own_ref, other_ref, out_ref):
     half = half_ref[0]
-    groups = spec_ref.shape[0]
-    for k in range(2):
-        for ref, place in ((own_ref, 2 * half + k), (other_ref, 2 * (1 - half) + k)):
-            total = None
-            for g in range(groups):
-                part = jnp.dot(
-                    spec_ref[g],
-                    ref[k, GROUP * g : GROUP * g + GROUP, :],
-                    preferred_element_type=jnp.float32,
-                )
-                total = part if total is None else total + part
-            out_ref[pl.ds(place, 1)] = total.astype(jnp.bfloat16)[None]
+    spectra = jnp.concatenate([spec_ref[g] for g in range(spec_ref.shape[0])], 1)
+    for ref, place in ((own_ref, 2 * half), (other_ref, 2 * (1 - half))):
+        weights = jnp.concatenate([ref[0], ref[1]], 1)
+        total = jnp.dot(spectra, weights, preferred_element_type=jnp.float32)
+        total = total.astype(jnp.bfloat16)
+        width = total.shape[1] // 2
+        for k in range(2):
+            out_ref[pl.ds(place + k, 1)] = total[:, width * k : width * k + width][None]
 
 
 def output_map(half, gathered, own, other):

time: 78.1 us -> 77.8 us (level)
  no operation moved by 1% of the time
where the time goes in v9:
time: 77.8 us; the launch traced here: 77.5 us
  blocking collectives  59.3 us (76%)
  starting transfers between devices  8.3 us (11%)
  Pallas kernels  6.09 us (8%)
  waiting for transfers between devices  3.04 us (4%)
    all_to_all x1, blocking collectives, local(): arrived = lax.all_to_all(projected, 'row', 0, 0, tiled=True)  22.9 us
    all_gather x1, blocking collectives, local(): gathered = lax.all_gather(mixed, 'g', axis=0)  16.2 us
    all_to_all x1, blocking collectives, local(): output = lax.all_to_all(output, ('h', 'k'), 0, 0, tiled=True)  10.5 us
    all_gather x1, blocking collectives, local(): lax.all_gather(arrived.reshape(2 * rows, 2, *arrived.shape[1:]), 'k', axi...  5.75 us
    all_to_all x1, starting transfers between devices, local(): arrived = lax.all_to_all(spectra, ('row', 'h'), 0, 0, tiled=True)  5.12 us
    all_gather x1, blocking collectives, local(): own = lax.all_gather(w_out, 'k', axis=0)  3.9 us
    pallas_call x1, Pallas kernels, project(): pl.pallas_call(project_body, in_specs=[pl.BlockSpec(memory_space=pltpu.HB...  3.42 us
    ppermute x1, starting transfers between devices, local(): other = lax.ppermute(own, 'h', [(0, 1), (1, 0)])  3.19 us
  transfers between devices with their start and end apart: 2, of which 1 were waited for; matrix products, arithmetic and copies ran while one was open for 0% of the time, Pallas kernels for 1%

profile of v9, /device:TPU:1, one launch (start us, length us, event | category | flops | bytes accessed | tf_op | source)
XLA Modules:
  0.0 77.5 jit_solution(3101585741148167889)
XLA Ops:
  0.0 0.0 copy-start.3
  0.0 0.0 copy-start.1
  0.0 0.0 copy-start.2
  0.0 0.0 copy-start
  0.0 0.0 copy-start.4
  0.0 3.4 %shard_map.82 = bf16[32,16,128]{2,1,0:T(8,128)(2,1)S(1)} custom-call(bf16[1024,2048]{1,0:T(8,128)(2,1)} %x_hbm.1, bf16[64,2048]{1,0:T(8,128)(2,1)} %bitcast.13, f32[1,2048]{1,0:T(1,128)} %bitcast.14), custom_call_target="tpu_custom_call" | custom-call | tf_op jit(solution)/shard_map/pallas_call | solution.py:70
  3.5 22.9 %all_to_all.15.x_ref = bf16[32,16,128]{2,1,0:T(8,128)(2,1)S(1)} all-to-all(bf16[32,16,128]{2,1,0:T(8,128)(2,1)S(1)} %shard_map.82), channel_id=1, replica_groups=mesh['row'=32,'g'=4,'h'=2,'k'=2] {'row'}, dimensions={0} | all-to-all | bytes 262144 | tf_op jit(solution)/shard_map/all_to_all | solution.py:215
  26.3 0.0 copy-done.3
  26.3 0.0 copy-done.1
  26.3 0.0 copy-done.2
  26.3 1.7 %shard_map.83 = bf16[128,8,128]{2,1,0:T(8,128)(2,1)} custom-call(bf16[32,16,128]{2,1,0:T(8,128)(2,1)S(1)} %all_to_all.15.x_ref, bf16[512,256]{1,0:T(8,128)(2,1)S(1)} %copy-done.2, f32[2,256,128]{2,1,0:T(8,128)S(1)} %copy-done.1, bf16[256,256]{1,0:T(8,128)(2,1)S(1)} %copy-done.3), custom_call_target="tpu_custom_call" | custom-call | tf_op jit(solution)/shard_map/pallas_call | solution.py:133
  28.0 5.1 %all-to-all-start.1 = ((bf16[128,8,128]{2,1,0:T(8,128)(2,1)}), bf16[128,8,128]{2,1,0:T(8,128)(2,1)S(1)}, u32[]{:S(2)}, u32[]{:S(2)}) async-start(bf16[128,8,128]{2,1,0:T(8,128)(2,1)} %shard_map.83), calls=%async_computation.1 | async-start | bytes 524288 | tf_op jit(solution)/shard_map/all_to_all | solution.py:217
  33.1 0.0 copy-done.4
  33.1 3.9 %all-gather.1 = bf16[2048,128]{1,0:T(8,128)(2,1)S(1)} all-gather(bf16[1024,128]{1,0:T(8,128)(2,1)S(1)} %copy-done.4), channel_id=3, replica_groups=mesh['row'=32,'g'=4,'h'=2,'k'=2] {'k'}, dimensions={0}, use_global_device_ids=true | all-gather | bytes 786432 | tf_op jit(solution)/shard_map/all_gather | solution.py:212
  37.0 3.2 %collective-permute-start = (bf16[2,1024,128]{2,1,0:T(8,128)(2,1)S(1)}, bf16[2,1024,128]{2,1,0:T(8,128)(2,1)S(1)}, u32[]{:S(2)}, u32[]{:S(2)}) collective-permute-start(bf16[2,1024,128]{2,1,0:T(8,128)(2,1)S(1)} %bitcast.9), channel_id=1, source_target_pairs={{0,2},{2,0},{1,3},{3,1},{4,6},{6,4},{5,7},{7,5},{8,10},{10,8},{9,1... | collective-permute-start | bytes 1572872 | tf_op jit(solution)/shard_map/ppermute | solution.py:213
  40.2 3.0 %all-to-all-done.1 = bf16[128,8,128]{2,1,0:T(8,128)(2,1)S(1)} async-done(((bf16[128,8,128]{2,1,0:T(8,128)(2,1)}), bf16[128,8,128]{2,1,0:T(8,128)(2,1)S(1)}, u32[]{:S(2)}, u32[]{:S(2)}) %all-to-all-start.1) | async-done | bytes 262176 | tf_op jit(solution)/shard_map/all_to_all | solution.py:217
  43.3 5.7 %all_gather.15.x_ref = bf16[2,64,2,8,128]{4,3,2,1,0:T(8,128)(2,1)S(1)} all-gather(bf16[1,64,2,8,128]{4,3,2,1,0:T(8,128)(2,1)S(1)} %bitcast.11), channel_id=1, replica_groups=mesh['row'=32,'g'=4,'h'=2,'k'=2] {'k'}, dimensions={0}, use_global_device_ids=true | all-gather | bytes 786432 | tf_op jit(solution)/shard_map/all_gather | solution.py:218
  49.0 0.0 copy-done
  49.0 0.6 shard_map.84
  49.6 16.2 %all-gather = bf16[1024,256]{1,0:T(8,128)(2,1)S(1)} all-gather(bf16[256,256]{1,0:T(8,128)(2,1)S(1)} %shard_map.84), channel_id=2, replica_groups=mesh['row'=32,'g'=4,'h'=2,'k'=2] {'g'}, dimensions={0}, use_global_device_ids=true | all-gather | bytes 655360 | tf_op jit(solution)/shard_map/all_gather | solution.py:221
  65.8 0.0 collective-permute-done.other_ref
  65.8 0.4 shard_map.85
  66.3 10.5 %all_to_all.16 = bf16[4,256,128]{2,1,0:T(8,128)(2,1)S(1)} all-to-all(bf16[4,256,128]{2,1,0:T(8,128)(2,1)S(1)} %shard_map.85), channel_id=1, replica_groups=mesh['row'=32,'g'=4,'h'=2,'k'=2] {'h','k'}, dimensions={0} | all-to-all | bytes 524288 | tf_op jit(solution)/shard_map/all_to_all | solution.py:224
  76.8 0.7 copy.10
Async XLA Ops:
  0.0 26.3 %copy-start.3 = (bf16[256,256]{1,0:T(8,128)(2,1)S(1)}, bf16[256,256]{1,0:T(8,128)(2,1)}, u32[]{:S(2)}) copy-start(bf16[256,256]{1,0:T(8,128)(2,1)} %constant.16.clone.two_ref) | copy-start | bytes 393220
  0.0 26.3 %copy-start.1 = (f32[2,256,128]{2,1,0:T(8,128)S(1)}, f32[2,256,128]{2,1,0:T(8,128)}, u32[]{:S(2)}) copy-start(f32[2,256,128]{2,1,0:T(8,128)} %constant.15.clone.turn_ref) | copy-start | bytes 786436
  0.0 26.3 %copy-start.2 = (bf16[512,256]{1,0:T(8,128)(2,1)S(1)}, bf16[512,256]{1,0:T(8,128)(2,1)}, u32[]{:S(2)}) copy-start(bf16[512,256]{1,0:T(8,128)(2,1)} %constant.14.clone.one_ref) | copy-start | bytes 786436
  0.0 49.0 %copy-start = (bf16[256,512]{1,0:T(8,128)(2,1)S(1)}, bf16[256,512]{1,0:T(8,128)(2,1)}, u32[]{:S(2)}) copy-start(bf16[256,512]{1,0:T(8,128)(2,1)} %constant.17.clone.table_ref) | copy-start | bytes 786436
  0.0 33.1 %copy-start.4 = (bf16[1024,128]{1,0:T(8,128)(2,1)S(1)}, bf16[1024,128]{1,0:T(8,128)(2,1)}, u32[]{:S(2)}) copy-start(bf16[1024,128]{1,0:T(8,128)(2,1)} %param.11) | copy-start | bytes 786436
  28.0 15.3 %all-to-all-start.1 = ((bf16[128,8,128]{2,1,0:T(8,128)(2,1)}), bf16[128,8,128]{2,1,0:T(8,128)(2,1)S(1)}, u32[]{:S(2)}, u32[]{:S(2)}) async-start(bf16[128,8,128]{2,1,0:T(8,128)(2,1)} %shard_map.83), calls=%async_computation.1 | async-start | bytes 524288 | tf_op jit(solution)/shard_map/all_to_all | solution.py:217
  37.0 28.8 %collective-permute-start = (bf16[2,1024,128]{2,1,0:T(8,128)(2,1)S(1)}, bf16[2,1024,128]{2,1,0:T(8,128)(2,1)S(1)}, u32[]{:S(2)}, u32[]{:S(2)}) collective-permute-start(bf16[2,1024,128]{2,1,0:T(8,128)(2,1)S(1)} %bitcast.9), channel_id=1, source_target_pairs={{0,2},{2,0},{1,3},{3,1},{4,6},{6,4},{5,7},{7,5},{8,10},{10,8},{9,1... | collective-permute-start | bytes 1572872 | tf_op jit(solution)/shard_map/ppermute | solution.py:213

commit v10 on v9

--- a/solution.py
+++ b/solution.py
@@ -104,24 +104,28 @@
 def positions_body(x_ref, one_ref, turn_ref, two_ref, out_ref, scr):
     wide = x_ref[...].astype(jnp.float32)
     n_first = wide.shape[0] * 8
-    both = [
-        wide[:, 8 * c : 8 * c + 8, :].reshape(n_first, BLOCK).astype(jnp.bfloat16)
-        for c in range(2)
-    ]
+    both = [wide[:, 8 * c : 8 * c + 8, :].reshape(n_first, BLOCK) for c in range(2)]
+    data = jnp.concatenate(both, 1).astype(jnp.bfloat16)
     cosine, sine = turn_ref[0], turn_ref[1]
+    y = jnp.dot(one_ref[...], data, preferred_element_type=jnp.float32)
+    turned = []
     for c in range(2):
-        y = jnp.dot(one_ref[...], both[c], preferred_element_type=jnp.float32)
-        y_cos, y_sin = y[:n_first], y[n_first:]
-        turned = jnp.concatenate(
-            [y_cos * cosine - y_sin * sine, -(y_sin * cosine) - y_cos * sine], 1
-        ).astype(jnp.bfloat16)
-        z = lax.dot_general(
-            two_ref[...], turned, (((1,), (1,)), ((), ())), preferred_element_type=jnp.float32
-        )
+        y_cos = y[:n_first, BLOCK * c : BLOCK * c + BLOCK]
+        y_sin = y[n_first:, BLOCK * c : BLOCK * c + BLOCK]
+        pair = [y_cos * cosine - y_sin * sine, -(y_sin * cosine) - y_cos * sine]
+        turned.append(jnp.concatenate(pair, 1).astype(jnp.bfloat16))
+    z = lax.dot_general(
+        two_ref[...],
+        jnp.concatenate(turned, 0),
+        (((1,), (1,)), ((), ())),
+        preferred_element_type=jnp.float32,
+    )
+    for c in range(2):
         for part in range(2):
             for high in range(2):
+                column = n_first * c + BLOCK * high
                 scr[:, 4 * c + 2 * part + high, :] = z[
-                    BLOCK * part : BLOCK * part + BLOCK, BLOCK * high : BLOCK * high + BLOCK
+                    BLOCK * part : BLOCK * part + BLOCK, column : column + BLOCK
                 ]
     out_ref[...] = scr[...].astype(jnp.bfloat16)
 

time: 77.8 us -> 77.6 us (level)
  no operation moved by 1% of the time
where the time goes in v10:
time: 77.6 us; the launch traced here: 77.3 us
  blocking collectives  59.3 us (76%)
  starting transfers between devices  8.31 us (11%)
  Pallas kernels  5.88 us (8%)
  waiting for transfers between devices  3.03 us (4%)
    all_to_all x1, blocking collectives, local(): arrived = lax.all_to_all(projected, 'row', 0, 0, tiled=True)  22.9 us
    all_gather x1, blocking collectives, local(): gathered = lax.all_gather(mixed, 'g', axis=0)  16.2 us
    all_to_all x1, blocking collectives, local(): output = lax.all_to_all(output, ('h', 'k'), 0, 0, tiled=True)  10.6 us
    all_gather x1, blocking collectives, local(): lax.all_gather(arrived.reshape(2 * rows, 2, *arrived.shape[1:]), 'k', axi...  5.75 us
    all_to_all x1, starting transfers between devices, local(): arrived = lax.all_to_all(spectra, ('row', 'h'), 0, 0, tiled=True)  5.12 us
    all_gather x1, blocking collectives, local(): own = lax.all_gather(w_out, 'k', axis=0)  3.9 us
    pallas_call x1, Pallas kernels, project(): pl.pallas_call(project_body, in_specs=[pl.BlockSpec(memory_space=pltpu.HB...  3.42 us
    ppermute x1, starting transfers between devices, local(): other = lax.ppermute(own, 'h', [(0, 1), (1, 0)])  3.19 us
  transfers between devices with their start and end apart: 2, of which 1 were waited for; matrix products, arithmetic and copies ran while one was open for 0% of the time, Pallas kernels for 1%

profile of v10, /device:TPU:1, one launch (start us, length us, event | category | flops | bytes accessed | tf_op | source)
XLA Modules:
  0.0 77.3 jit_solution(11121569464832530650)
XLA Ops:
  0.0 0.0 copy-start.3
  0.0 0.0 copy-start.1
  0.0 0.0 copy-start.2
  0.0 0.0 copy-start
  0.0 0.0 copy-start.4
  0.0 3.4 %shard_map.82 = bf16[32,16,128]{2,1,0:T(8,128)(2,1)S(1)} custom-call(bf16[1024,2048]{1,0:T(8,128)(2,1)} %x_hbm.1, bf16[64,2048]{1,0:T(8,128)(2,1)} %bitcast.13, f32[1,2048]{1,0:T(1,128)} %bitcast.14), custom_call_target="tpu_custom_call" | custom-call | tf_op jit(solution)/shard_map/pallas_call | solution.py:70
  3.5 22.9 %all_to_all.15.x_ref = bf16[32,16,128]{2,1,0:T(8,128)(2,1)S(1)} all-to-all(bf16[32,16,128]{2,1,0:T(8,128)(2,1)S(1)} %shard_map.82), channel_id=1, replica_groups=mesh['row'=32,'g'=4,'h'=2,'k'=2] {'row'}, dimensions={0} | all-to-all | bytes 262144 | tf_op jit(solution)/shard_map/all_to_all | solution.py:219
  26.3 0.0 copy-done.3
  26.3 0.0 copy-done.1
  26.3 0.0 copy-done.2
  26.3 1.5 %shard_map.83 = bf16[128,8,128]{2,1,0:T(8,128)(2,1)} custom-call(bf16[32,16,128]{2,1,0:T(8,128)(2,1)S(1)} %all_to_all.15.x_ref, bf16[512,256]{1,0:T(8,128)(2,1)S(1)} %copy-done.2, f32[2,256,128]{2,1,0:T(8,128)S(1)} %copy-done.1, bf16[256,256]{1,0:T(8,128)(2,1)S(1)} %copy-done.3), custom_call_target="tpu_custom_call" | custom-call | tf_op jit(solution)/shard_map/pallas_call | solution.py:137
  27.8 5.1 %all-to-all-start.1 = ((bf16[128,8,128]{2,1,0:T(8,128)(2,1)}), bf16[128,8,128]{2,1,0:T(8,128)(2,1)S(1)}, u32[]{:S(2)}, u32[]{:S(2)}) async-start(bf16[128,8,128]{2,1,0:T(8,128)(2,1)} %shard_map.83), calls=%async_computation.1 | async-start | bytes 524288 | tf_op jit(solution)/shard_map/all_to_all | solution.py:221
  32.9 0.0 copy-done.4
  32.9 3.9 %all-gather.1 = bf16[2048,128]{1,0:T(8,128)(2,1)S(1)} all-gather(bf16[1024,128]{1,0:T(8,128)(2,1)S(1)} %copy-done.4), channel_id=3, replica_groups=mesh['row'=32,'g'=4,'h'=2,'k'=2] {'k'}, dimensions={0}, use_global_device_ids=true | all-gather | bytes 786432 | tf_op jit(solution)/shard_map/all_gather | solution.py:216
  36.8 3.2 %collective-permute-start = (bf16[2,1024,128]{2,1,0:T(8,128)(2,1)S(1)}, bf16[2,1024,128]{2,1,0:T(8,128)(2,1)S(1)}, u32[]{:S(2)}, u32[]{:S(2)}) collective-permute-start(bf16[2,1024,128]{2,1,0:T(8,128)(2,1)S(1)} %bitcast.9), channel_id=1, source_target_pairs={{0,2},{2,0},{1,3},{3,1},{4,6},{6,4},{5,7},{7,5},{8,10},{10,8},{9,1... | collective-permute-start | bytes 1572872 | tf_op jit(solution)/shard_map/ppermute | solution.py:217
  40.0 3.0 %all-to-all-done.1 = bf16[128,8,128]{2,1,0:T(8,128)(2,1)S(1)} async-done(((bf16[128,8,128]{2,1,0:T(8,128)(2,1)}), bf16[128,8,128]{2,1,0:T(8,128)(2,1)S(1)}, u32[]{:S(2)}, u32[]{:S(2)}) %all-to-all-start.1) | async-done | bytes 262176 | tf_op jit(solution)/shard_map/all_to_all | solution.py:221
  43.1 5.8 %all_gather.15.x_ref = bf16[2,64,2,8,128]{4,3,2,1,0:T(8,128)(2,1)S(1)} all-gather(bf16[1,64,2,8,128]{4,3,2,1,0:T(8,128)(2,1)S(1)} %bitcast.11), channel_id=1, replica_groups=mesh['row'=32,'g'=4,'h'=2,'k'=2] {'k'}, dimensions={0}, use_global_device_ids=true | all-gather | bytes 786432 | tf_op jit(solution)/shard_map/all_gather | solution.py:222
  48.8 0.0 copy-done
  48.8 0.6 shard_map.84
  49.4 16.2 %all-gather = bf16[1024,256]{1,0:T(8,128)(2,1)S(1)} all-gather(bf16[256,256]{1,0:T(8,128)(2,1)S(1)} %shard_map.84), channel_id=2, replica_groups=mesh['row'=32,'g'=4,'h'=2,'k'=2] {'g'}, dimensions={0}, use_global_device_ids=true | all-gather | bytes 655360 | tf_op jit(solution)/shard_map/all_gather | solution.py:225
  65.6 0.0 collective-permute-done.other_ref
  65.6 0.4 shard_map.85
  66.1 10.6 %all_to_all.16 = bf16[4,256,128]{2,1,0:T(8,128)(2,1)S(1)} all-to-all(bf16[4,256,128]{2,1,0:T(8,128)(2,1)S(1)} %shard_map.85), channel_id=1, replica_groups=mesh['row'=32,'g'=4,'h'=2,'k'=2] {'h','k'}, dimensions={0} | all-to-all | bytes 524288 | tf_op jit(solution)/shard_map/all_to_all | solution.py:228
  76.6 0.7 copy.10
Async XLA Ops:
  0.0 26.3 %copy-start.3 = (bf16[256,256]{1,0:T(8,128)(2,1)S(1)}, bf16[256,256]{1,0:T(8,128)(2,1)}, u32[]{:S(2)}) copy-start(bf16[256,256]{1,0:T(8,128)(2,1)} %constant.16.clone.two_ref) | copy-start | bytes 393220
  0.0 26.3 %copy-start.1 = (f32[2,256,128]{2,1,0:T(8,128)S(1)}, f32[2,256,128]{2,1,0:T(8,128)}, u32[]{:S(2)}) copy-start(f32[2,256,128]{2,1,0:T(8,128)} %constant.15.clone.turn_ref) | copy-start | bytes 786436
  0.0 26.3 %copy-start.2 = (bf16[512,256]{1,0:T(8,128)(2,1)S(1)}, bf16[512,256]{1,0:T(8,128)(2,1)}, u32[]{:S(2)}) copy-start(bf16[512,256]{1,0:T(8,128)(2,1)} %constant.14.clone.one_ref) | copy-start | bytes 786436
  0.0 48.8 %copy-start = (bf16[256,512]{1,0:T(8,128)(2,1)S(1)}, bf16[256,512]{1,0:T(8,128)(2,1)}, u32[]{:S(2)}) copy-start(bf16[256,512]{1,0:T(8,128)(2,1)} %constant.17.clone.table_ref) | copy-start | bytes 786436
  0.0 32.9 %copy-start.4 = (bf16[1024,128]{1,0:T(8,128)(2,1)S(1)}, bf16[1024,128]{1,0:T(8,128)(2,1)}, u32[]{:S(2)}) copy-start(bf16[1024,128]{1,0:T(8,128)(2,1)} %param.11) | copy-start | bytes 786436
  27.8 15.3 %all-to-all-start.1 = ((bf16[128,8,128]{2,1,0:T(8,128)(2,1)}), bf16[128,8,128]{2,1,0:T(8,128)(2,1)S(1)}, u32[]{:S(2)}, u32[]{:S(2)}) async-start(bf16[128,8,128]{2,1,0:T(8,128)(2,1)} %shard_map.83), calls=%async_computation.1 | async-start | bytes 524288 | tf_op jit(solution)/shard_map/all_to_all | solution.py:221
  36.8 28.8 %collective-permute-start = (bf16[2,1024,128]{2,1,0:T(8,128)(2,1)S(1)}, bf16[2,1024,128]{2,1,0:T(8,128)(2,1)S(1)}, u32[]{:S(2)}, u32[]{:S(2)}) collective-permute-start(bf16[2,1024,128]{2,1,0:T(8,128)(2,1)S(1)} %bitcast.9), channel_id=1, source_target_pairs={{0,2},{2,0},{1,3},{3,1},{4,6},{6,4},{5,7},{7,5},{8,10},{10,8},{9,1... | collective-permute-start | bytes 1572872 | tf_op jit(solution)/shard_map/ppermute | solution.py:217
